TPU v7x, 32 devices: a whole 2x2x4 slice. The times are simulated.
32 devices in a mesh: ep: 8 (over z, x), tp: 4 (over y, core).
Axes of the slice: x: 2, y: 2, z: 4, core: 2. Of those that a mesh axis runs over, the one named last changes fastest.
Arguments:
- tokens: bfloat16 [128, 2048], P('ep'), may hold values from -6 to 6
- lengths: int32 [128], P('ep'), may hold values from 1 to 1024, as said below
- key_cache: bfloat16 [128, 1024, 8, 128], P('ep', None, 'tp'), may hold values from -200 to 200
- value_cache: bfloat16 [128, 1024, 8, 128], P('ep', None, 'tp'), may hold values from -6 to 6
- attn_gain: float32 [2048], replicated, may hold values from 0.1 to 1.9
- w_query: bfloat16 [2048, 8, 128], P(None, 'tp'), may hold values from -0.1875 to 0.1875
- w_key: bfloat16 [2048, 8, 128], P(None, 'tp'), may hold values from -0.15625 to 0.15625
- w_value: bfloat16 [2048, 8, 128], P(None, 'tp'), may hold values from -0.125 to 0.125
- mix_lambda: float32 [8], P('tp'), may hold values from 0.3 to 0.8
- head_gain: float32 [128], replicated, may hold values from 0.1 to 1.9
- w_out: bfloat16 [8, 128, 2048], P('tp'), may hold values from -2.5 to 2.5
- ffn_gain: float32 [2048], replicated, may hold values from 0.1 to 1.9
- w_gate: bfloat16 [8, 2048, 2048], P('ep', None, 'tp'), may hold values from -1 to 1
- w_up: bfloat16 [8, 2048, 2048], P('ep', None, 'tp'), may hold values from -1 to 1
- w_down: bfloat16 [8, 2048, 2048], P('ep', 'tp'), may hold values from -0.046875 to 0.046875
- routes: int32 [128, 4], P('ep'), may hold values from 0 to 7, all different within a row; in each aligned block of 16 rows (0 to 15, 16 to 31, ...) at most 16 rows name the same one
- route_weights: float32 [128, 4], P('ep'), may hold values from 0.1 to 1
Outputs:
- mixed: bfloat16 [128, 2048], P('ep', 'tp')
Inputs may be any that keep to these rules, and one draw needn't show every extreme that they name: `routes`: in each aligned block of 16 rows no expert is named by more than 16 entries, and one is named by exactly 16 in some block; each row names 4 different experts. `lengths`: some sequence has all 1024 positions valid.
All inputs are finite; a program needn't handle non-finite values.
Results may differ from a plain program's by a relative error of at most 0.02.
The roundings to bfloat16 on the way count: a program that leaves them out, or rounds other values in their place, can miss the bound.
Values may be sent and summed in bfloat16 or wider, within the bound.
A program may use at most 128 MiB of HBM per device.

v0:
```python
import functools
import math

import jax
import jax.numpy as jnp
from jax import lax
from jax.experimental import pallas as pl
from jax.experimental.pallas import tpu as pltpu
from jax.sharding import PartitionSpec as P

epsilon = 1e-06
clamp_limit = 7.0
sigmoid_slope = 1.702
branch_scale = 0.2


def norm_rows(source, gain):
    wide = source.astype(jnp.float32)
    return wide * lax.rsqrt(jnp.mean(wide * wide, axis=-1, keepdims=True) + epsilon) * gain


def attend_kernel(
    group_heads,
    score_scale,
    lengths_ref,
    lambda_ref,
    query_ref,
    key_new_ref,
    value_new_ref,
    gain_ref,
    key_ref,
    value_ref,
    out_ref,
):
    batch, maps, head_width = query_ref.shape
    flat_len = key_ref.shape[1]
    scores = jnp.concatenate(
        [
            lax.dot_general(
                query_ref[i], key_ref[i], (((1,), (1,)), ((), ())), preferred_element_type=jnp.float32
            )
            for i in range(batch)
        ],
        axis=0,
    )
    scores = scores * score_scale
    own = jnp.concatenate(
        [
            jnp.sum(
                query_ref[i].astype(jnp.float32) * key_new_ref[i].astype(jnp.float32),
                axis=-1,
                keepdims=True,
            )
            for i in range(batch)
        ],
        axis=0,
    )
    own = own * score_scale
    rows = lax.broadcasted_iota(jnp.int32, (batch * maps, 1), 0)
    limit = jnp.zeros((batch * maps, 1), jnp.int32)
    for i in range(batch):
        length = lengths_ref[pl.program_id(0) * batch + i]
        limit = jnp.where(rows // maps == i, length * group_heads, limit)
    column = lax.broadcasted_iota(jnp.int32, (batch * maps, flat_len), 1)
    row_head = lax.rem(rows, maps) // 2
    live = (column < limit) & (lax.rem(column, group_heads) == row_head)
    scores = jnp.where(live, scores, -jnp.inf)
    peak = jnp.maximum(jnp.max(scores, axis=-1, keepdims=True), own)
    weights = jnp.exp(scores - peak)
    own_weight = jnp.exp(own - peak)
    denominator = jnp.sum(weights, axis=-1, keepdims=True) + own_weight
    shares = weights / denominator
    own_share = own_weight / denominator
    for i in range(batch):
        mixed, own_mixed = [], []
        for h in range(group_heads):
            first = i * maps + 2 * h
            balance = lambda_ref[h]
            mixed.append(shares[first : first + 1] - balance * shares[first + 1 : first + 2])
            own_mixed.append(
                own_share[first : first + 1] - balance * own_share[first + 1 : first + 2]
            )
        mix_weights = jnp.concatenate(mixed, axis=0).astype(jnp.bfloat16)
        own_mix = jnp.concatenate(own_mixed, axis=0).astype(jnp.bfloat16).astype(jnp.float32)
        heads_out = jnp.dot(mix_weights, value_ref[i], preferred_element_type=jnp.float32)
        heads_out += own_mix * value_new_ref[i].astype(jnp.float32)
        scale = lax.rsqrt(jnp.mean(heads_out * heads_out, axis=-1, keepdims=True) + epsilon)
        out_ref[i] = (heads_out * scale * gain_ref[...] * branch_scale).astype(jnp.bfloat16)


MESH = pl.DeviceIdType.MESH


def exchange_kernel(
    n_ep,
    n_tp,
    heads_ref,
    tokens_ref,
    gain_ref,
    routes_ref,
    route_weights_ref,
    w_out_hbm,
    w_gate_hbm,
    w_up_hbm,
    w_down_hbm,
    out_ref,
    w_out_ref,
    w_gate_ref,
    w_up_ref,
    w_down_ref,
    part_ref,
    part_in_ref,
    rows_ref,
    normed_ref,
    piece_ref,
    piece_in_ref,
    back_ref,
    back_in_ref,
    weight_sems,
    part_sems,
    rows_sems,
    fan_sems,
    piece_sems,
    back_sems,
):
    my_ep, my_tp = lax.axis_index("ep"), lax.axis_index("tp")
    seq_dev = tokens_ref.shape[0]
    block = out_ref.shape[1]

    weight_pairs = (
        (w_out_hbm, w_out_ref),
        (w_gate_hbm, w_gate_ref),
        (w_up_hbm, w_up_ref),
        (w_down_hbm, w_down_ref),
    )
    weight_copies = [
        pltpu.make_async_copy(source, target, weight_sems.at[i])
        for i, (source, target) in enumerate(weight_pairs)
    ]
    for copy in weight_copies:
        copy.start()

    barrier = pltpu.get_barrier_semaphore()

    for k in range(1, n_ep):
        pl.semaphore_signal(
            barrier, inc=1, device_id=(lax.rem(my_ep + k, n_ep), my_tp), device_id_type=MESH
        )
    for k in range(1, n_tp):
        pl.semaphore_signal(
            barrier, inc=1, device_id=(my_ep, lax.rem(my_tp + k, n_tp)), device_id_type=MESH
        )

    weight_copies[0].wait()
    for c in range(n_tp):
        columns = slice(c * block, (c + 1) * block)
        part_ref[c] = jnp.dot(
            heads_ref[...], w_out_ref[:, columns], preferred_element_type=jnp.float32
        ).astype(jnp.bfloat16)
    pl.semaphore_wait(barrier, n_ep + n_tp - 2)

    for k in range(1, n_tp):
        peer = lax.rem(my_tp + k, n_tp)
        pltpu.make_async_remote_copy(
            src_ref=part_ref.at[peer],
            dst_ref=part_in_ref.at[k - 1],
            send_sem=part_sems.at[0],
            recv_sem=part_sems.at[1],
            device_id=(my_ep, peer),
            device_id_type=MESH,
        ).start()
    own_columns = pl.ds(pl.multiple_of(my_tp * block, block), block)
    own_rows = pl.ds(pl.multiple_of(my_ep * seq_dev, seq_dev), seq_dev)
    attention = part_ref[my_tp].astype(jnp.float32)
    if n_tp > 1:
        pltpu.make_async_copy(part_in_ref, part_in_ref, part_sems.at[1]).wait()
        for k in range(1, n_tp):
            attention += part_in_ref[k - 1].astype(jnp.float32)
    residual = (tokens_ref[:, own_columns].astype(jnp.float32) + attention).astype(jnp.bfloat16)
    rows_ref[own_rows, own_columns] = residual

    far_first = sorted(range(1, n_ep), key=lambda k: -min(k, n_ep - k))

    def rows_copy(source_ep, device, sems, recv):
        place = rows_ref.at[
            pl.ds(pl.multiple_of(source_ep * seq_dev, seq_dev), seq_dev), own_columns
        ]
        return pltpu.make_async_remote_copy(
            src_ref=place,
            dst_ref=place,
            send_sem=sems.at[0],
            recv_sem=sems.at[recv],
            device_id=device,
            device_id_type=MESH,
        )

    for k in far_first:
        rows_copy(my_ep, (lax.rem(my_ep + k, n_ep), my_tp), rows_sems, k).start()
    for k in [0] + far_first[::-1]:
        source_ep = lax.rem(my_ep + n_ep - k, n_ep)
        if k:
            rows_copy(source_ep, (my_ep, my_tp), rows_sems, k).wait_recv()
        for j in range(1, n_tp):
            peer = lax.rem(my_tp + j, n_tp)
            rows_copy(source_ep, (my_ep, peer), fan_sems, 1).start()
    if n_tp > 1:
        pltpu.make_async_copy(piece_in_ref, piece_in_ref, fan_sems.at[1]).wait()
    wide = rows_ref[...].astype(jnp.float32)
    scale = lax.rsqrt(jnp.mean(wide * wide, axis=-1, keepdims=True) + epsilon)
    normed_ref[...] = (wide * scale * gain_ref[...]).astype(jnp.bfloat16)

    weight_copies[1].wait()
    gate_value = jnp.minimum(
        jnp.dot(normed_ref[...], w_gate_ref[...], preferred_element_type=jnp.float32), clamp_limit
    )
    weight_copies[2].wait()
    up_value = jnp.clip(
        jnp.dot(normed_ref[...], w_up_ref[...], preferred_element_type=jnp.float32),
        -clamp_limit,
        clamp_limit,
    )
    activated = ((up_value + 1.0) * gate_value * jax.nn.sigmoid(sigmoid_slope * gate_value)).astype(
        jnp.bfloat16
    )
    weight_copies[3].wait()

    targets = far_first + [0]
    for j in sorted(range(1, n_tp), key=lambda j: -min(j, n_tp - j)) + [0]:
        peer = lax.rem(my_tp + j, n_tp)
        columns = pl.ds(pl.multiple_of(peer * block, block), block)
        piece = jnp.dot(
            activated, w_down_ref[:, columns], preferred_element_type=jnp.float32
        ).astype(jnp.bfloat16)
        piece_ref[j] = piece.reshape(n_ep, seq_dev, block)
        if j:
            for k in targets:
                target_ep = lax.rem(my_ep + k, n_ep)
                pltpu.make_async_remote_copy(
                    src_ref=piece_ref.at[j, target_ep],
                    dst_ref=piece_in_ref.at[target_ep, j - 1],
                    send_sem=fan_sems.at[2],
                    recv_sem=piece_sems.at[k],
                    device_id=(my_ep, peer),
                    device_id_type=MESH,
                ).start()

    for k in targets:
        target_ep = lax.rem(my_ep + k, n_ep)
        summed = piece_ref[0, target_ep].astype(jnp.float32)
        if n_tp > 1:
            landed = piece_in_ref.at[target_ep]
            pltpu.make_async_copy(landed, landed, piece_sems.at[k]).wait()
            for j in range(1, n_tp):
                summed += piece_in_ref[target_ep, j - 1].astype(jnp.float32)
        back_ref[k] = summed.astype(jnp.bfloat16)
        if k:
            pltpu.make_async_remote_copy(
                src_ref=back_ref.at[k],
                dst_ref=back_in_ref.at[k - 1],
                send_sem=back_sems.at[0],
                recv_sem=back_sems.at[k],
                device_id=(target_ep, my_tp),
                device_id_type=MESH,
            ).start()

    total = rows_ref[own_rows, own_columns].astype(jnp.float32)
    eye = lax.broadcasted_iota(jnp.int32, (seq_dev, seq_dev), 0) == lax.broadcasted_iota(
        jnp.int32, (seq_dev, seq_dev), 1
    )
    for k in [0] + far_first[::-1]:
        expert = lax.rem(my_ep + n_ep - k, n_ep)
        named = jnp.where(routes_ref[...] == expert, route_weights_ref[...], 0.0)
        weight = jnp.sum(named, axis=0, keepdims=True)
        weight = jnp.sum(jnp.where(eye, weight, 0.0), axis=1, keepdims=True)
        if k:
            arrived = back_in_ref.at[k - 1]
            pltpu.make_async_copy(arrived, arrived, back_sems.at[k]).wait()
            total += weight * back_in_ref[k - 1].astype(jnp.float32)
        else:
            total += weight * back_ref[0].astype(jnp.float32)
    out_ref[...] = total.astype(jnp.bfloat16)
    if n_ep > 1:
        pltpu.make_async_copy(back_in_ref, back_in_ref, rows_sems.at[0]).wait()
        pltpu.make_async_copy(back_in_ref, back_in_ref, back_sems.at[0]).wait()
    if n_tp > 1:
        pltpu.make_async_copy(part_in_ref, part_in_ref, part_sems.at[0]).wait()
        pltpu.make_async_copy(piece_in_ref, piece_in_ref, fan_sems.at[0]).wait()
        pltpu.make_async_copy(piece_in_ref, piece_in_ref, fan_sems.at[2]).wait()


def exchange_layer(
    heads, tokens, w_out, ffn_gain, routes, route_weights, w_gate, w_up, w_down
):
    n_ep, n_tp = lax.axis_size("ep"), lax.axis_size("tp")
    seq_dev, model_width = tokens.shape
    block = model_width // n_tp
    vmem = pl.BlockSpec(memory_space=pltpu.VMEM)
    anywhere = pl.BlockSpec(memory_space=pl.ANY)
    bf16 = jnp.bfloat16
    return pl.pallas_call(
        functools.partial(exchange_kernel, n_ep, n_tp),
        out_shape=jax.ShapeDtypeStruct((seq_dev, block), bf16),
        in_specs=[vmem] * 5 + [anywhere] * 4,
        out_specs=vmem,
        scratch_shapes=[
            pltpu.VMEM(w_out.shape, bf16),
            pltpu.VMEM(w_gate.shape, bf16),
            pltpu.VMEM(w_up.shape, bf16),
            pltpu.VMEM(w_down.shape, bf16),
            pltpu.VMEM((n_tp, seq_dev, block), bf16),
            pltpu.VMEM((max(n_tp - 1, 1), seq_dev, block), bf16),
            pltpu.VMEM((n_ep * seq_dev, model_width), bf16),
            pltpu.VMEM((n_ep * seq_dev, model_width), bf16),
            pltpu.VMEM((n_tp, n_ep, seq_dev, block), bf16),
            pltpu.VMEM((n_ep, max(n_tp - 1, 1), seq_dev, block), bf16),
            pltpu.VMEM((n_ep, seq_dev, block), bf16),
            pltpu.VMEM((max(n_ep - 1, 1), seq_dev, block), bf16),
            pltpu.SemaphoreType.DMA((4,)),
            pltpu.SemaphoreType.DMA((2,)),
            pltpu.SemaphoreType.DMA((n_ep,)),
            pltpu.SemaphoreType.DMA((3,)),
            pltpu.SemaphoreType.DMA((n_ep,)),
            pltpu.SemaphoreType.DMA((n_ep,)),
        ],
        compiler_params=pltpu.CompilerParams(collective_id=0, has_side_effects=True),
    )(heads, tokens, ffn_gain, routes, route_weights, w_out, w_gate, w_up, w_down)


def per_device(
    tokens,
    lengths,
    key_cache,
    value_cache,
    attn_gain,
    w_query,
    w_key,
    w_value,
    mix_lambda,
    head_gain,
    w_out,
    ffn_gain,
    w_gate,
    w_up,
    w_down,
    routes,
    route_weights,
):
    seq_dev, model_width = tokens.shape
    group_heads = w_query.shape[1]
    head_width = w_query.shape[2]
    half_width = head_width // 2
    columns = group_heads * head_width
    cache_len = key_cache.shape[1]
    normed = norm_rows(tokens, attn_gain).astype(jnp.bfloat16)
    queries = (
        jnp.dot(normed, w_query.reshape(model_width, columns), preferred_element_type=jnp.float32)
        .astype(jnp.bfloat16)
        .reshape(seq_dev, group_heads, head_width)
    )
    key_new = (
        jnp.dot(normed, w_key.reshape(model_width, columns), preferred_element_type=jnp.float32)
        .astype(jnp.bfloat16)
        .reshape(seq_dev, group_heads, head_width)
    )
    value_new = (
        jnp.dot(normed, w_value.reshape(model_width, columns), preferred_element_type=jnp.float32)
        .astype(jnp.bfloat16)
        .reshape(seq_dev, group_heads, head_width)
    )
    halves = (lax.iota(jnp.int32, head_width) < half_width).astype(jnp.bfloat16)
    stacked_query = jnp.stack([queries * halves, queries * (1 - halves)], axis=2)
    maps = 2 * group_heads
    flat_len = cache_len * group_heads
    batch = math.gcd(seq_dev, 4)
    smem = pl.BlockSpec(memory_space=pltpu.SMEM)
    per_seq = lambda rows: pl.BlockSpec((batch, rows, head_width), lambda i: (i, 0, 0))
    normed_heads = pl.pallas_call(
        functools.partial(attend_kernel, group_heads, half_width ** (-0.5)),
        grid=(seq_dev // batch,),
        out_shape=jax.ShapeDtypeStruct((seq_dev, group_heads, head_width), jnp.bfloat16),
        in_specs=[
            smem,
            smem,
            per_seq(maps),
            per_seq(maps),
            per_seq(group_heads),
            pl.BlockSpec((1, head_width), lambda i: (0, 0)),
            per_seq(flat_len),
            per_seq(flat_len),
        ],
        out_specs=per_seq(group_heads),
    )(
        lengths,
        mix_lambda,
        stacked_query.reshape(seq_dev, maps, head_width),
        jnp.repeat(key_new, 2, axis=1),
        value_new,
        head_gain.reshape(1, head_width),
        key_cache.reshape(seq_dev, flat_len, head_width),
        value_cache.reshape(seq_dev, flat_len, head_width),
    )
    return exchange_layer(
        normed_heads.reshape(seq_dev, columns),
        tokens,
        w_out.reshape(columns, model_width),
        ffn_gain.reshape(1, model_width),
        routes.T,
        route_weights.T,
        w_gate[0],
        w_up[0],
        w_down[0],
    )


def solution(mesh):
    placed = (
        P("ep", None),
        P("ep"),
        P("ep", None, "tp", None),
        P("ep", None, "tp", None),
        P(),
        P(None, "tp", None),
        P(None, "tp", None),
        P(None, "tp", None),
        P("tp"),
        P(),
        P("tp", None, None),
        P(),
        P("ep", None, "tp"),
        P("ep", None, "tp"),
        P("ep", "tp", None),
        P("ep", None),
        P("ep", None),
    )
    return jax.shard_map(
        per_device, mesh=mesh, in_specs=placed, out_specs=P("ep", "tp"), check_vma=False
    )
```

profile of v0, /device:TPU:0, one launch (start us, length us, event | category | flops | bytes accessed | tf_op | source)
XLA Modules:
  0.0 53.3 jit_solution(2712061715381479996)
XLA Ops:
  0.0 0.0 copy-start
  0.0 0.0 copy-start.2
  0.0 0.0 copy-start.1
  0.0 1.1 %fusion.6 = f32[16]{0:T(128)S(1)} fusion(bf16[16,2048]{1,0:T(8,128)(2,1)} %tokens_ref.1), kind=kLoop, calls=%fused_computation.11 | loop fusion | flops 98288 | bytes 65600 | tf_op jit(solution)/shard_map/reduce_sum | solution.py:19
  1.1 1.6 %convolution_convert_fusion.2 = bf16[16,256]{1,0:T(8,128)(2,1)S(1)} fusion(bf16[256,8,2,128]{3,2,1,0:T(2,128)(2,1)} %bitcast.42, bf16[16,2048]{1,0:T(8,128)(2,1)} %tokens_ref.1, f32[2048]{0:T(1024)} %param.21, f32[16]{0:T(128)S(1)} %add_rsqrt_fusion), kind=kOutput, calls=%fused_computation.2 | convolution fusion | flops 16912384 | bytes 1130560 | tf_op jit(solution)/shard_map/dot_general | solution.py:356
  2.7 0.6 %pad_maximum_fusion = bf16[16,2,2,128]{3,2,1,0:T(2,128)(2,1)} fusion(bf16[16,2,1,128]{3,2,1,0:T(2,128)(2,1)S(1)} %get-tuple-element.6, bf16[16,2,1,128]{3,2,1,0:T(2,128)(2,1)S(1)} %get-tuple-element.5), kind=kLoop, calls=%fused_computation.14 | loop fusion | flops 32768 | bytes 32768 | tf_op jit(solution)/shard_map/stack | solution.py:371
  3.4 1.6 %convolution_convert_fusion.1 = bf16[16,256]{1,0:T(8,128)(2,1)S(1)} fusion(bf16[256,8,2,128]{3,2,1,0:T(2,128)(2,1)} %bitcast.43, bf16[16,2048]{1,0:T(8,128)(2,1)} %tokens_ref.1, f32[2048]{0:T(1024)} %param.21, f32[16]{0:T(128)S(1)} %add_rsqrt_fusion), kind=kOutput, calls=%fused_computation.1 | convolution fusion | flops 16912384 | bytes 1130560 | tf_op jit(solution)/shard_map/dot_general | solution.py:361
  5.0 0.6 %broadcast_in_dim.2 = bf16[16,2,2,128]{3,2,1,0:T(2,128)(2,1)} broadcast(bf16[16,2,128]{2,1,0:T(2,128)(2,1)S(1)} %reshape.83), dimensions={0,1,3} | broadcast | bytes 24576 | tf_op jit(solution)/shard_map/broadcast_in_dim | solution.py:396
  5.6 0.0 copy-done
  5.6 0.0 copy-done.2
  5.6 0.0 copy-done.1
  5.6 0.3 convolution_convert_fusion
  5.9 0.6 %reshape.86.value_new_ref = bf16[16,2,128]{2,1,0:T(2,128)(2,1)} reshape(bf16[16,256]{1,0:T(8,128)(2,1)S(1)} %convolution_convert_fusion) | data formatting | bytes 16384 | tf_op jit(solution)/shard_map/reshape | solution.py:368
  6.5 9.6 %shard_map.163 = bf16[16,2,128]{2,1,0:T(2,128)(2,1)} custom-call(s32[16]{0:T(128)} %lengths_ref.1, f32[2]{0:T(128)} %lambda_ref.1, bf16[16,4,128]{2,1,0:T(4,128)(2,1)} %bitcast.34, bf16[16,4,128]{2,1,0:T(4,128)(2,1)} %bitcast.35, bf16[16,2,128]{2,1,0:T(2,128)(2,1)} %reshape.86.value_new_ref, f32[1,128]{1,0:T(1,128)} %bitcast.41, ...), custom_call_target="tpu_custom_call" | custom-call | tf_op jit(solution)/shard_map/pallas_call | solution.py:377
  16.1 1.3 %copy.37 = bf16[2,8,2,128]{3,1,2,0:T(8,128)(2,1)} copy(bf16[2,8,2,128]{3,2,1,0:T(2,128)(2,1)} %bitcast.36) | data formatting | bytes 16384
  17.4 34.6 %shard_map.164 = bf16[16,512]{1,0:T(8,128)(2,1)} custom-call(bf16[16,256]{1,0:T(8,128)(2,1)} %bitcast.37, bf16[16,2048]{1,0:T(8,128)(2,1)} %tokens_ref.1, f32[1,2048]{1,0:T(1,128)} %bitcast.38, s32[4,16]{1,0:T(4,128)} %bitcast.39, f32[4,16]{1,0:T(4,128)} %bitcast.40, bf16[256,2048]{1,0:T(8,128)(2,1)} %bitcast.33, bf16[2048,512]{1,0:T(8,128)(2,1)} %bitcast.30, ...), custom_call_target="tpu_custom_call" | custom-call | tf_op jit(solution)/shard_map/pallas_call | solution.py:300
  52.0 1.3 %copy.39 = bf16[16,512]{1,0:T(8,128)(2,1)} copy(bf16[16,512]{1,0:T(8,128)(2,1)} %shard_map.164) | data formatting | bytes 32768
  (6 shorter events, 0.1 us)
Async XLA Ops:
  0.0 5.6 %copy-start = (bf16[16,2048]{1,0:T(8,128)(2,1)S(1)}, bf16[16,2048]{1,0:T(8,128)(2,1)}, u32[]{:S(2)}) copy-start(bf16[16,2048]{1,0:T(8,128)(2,1)} %tokens_ref.1) | copy-start | bytes 196612
  0.0 5.6 %copy-start.2 = (f32[2048]{0:T(1024)S(1)}, f32[2048]{0:T(1024)}, u32[]{:S(2)}) copy-start(f32[2048]{0:T(1024)} %param.21) | copy-start | bytes 24580
  0.0 5.6 %copy-start.1 = (bf16[2048,2,128]{2,1,0:T(2,128)(2,1)S(1)}, bf16[2048,2,128]{2,1,0:T(2,128)(2,1)}, u32[]{:S(2)}) copy-start(bf16[2048,2,128]{2,1,0:T(2,128)(2,1)} %param.24) | copy-start | bytes 3145732
where the time goes:
time: 53.6 us; the launch traced here: 53.3 us
  Pallas kernels  44.2 us (82%)
  local copies, waits for them, and re-layouts  3.89 us (7%)
  matrix products  3.44 us (6%)
  other arithmetic  1.76 us (3%)
    pallas_call x1, Pallas kernels, exchange_layer(): pl.pallas_call(functools.partial(exchange_kernel, n_ep, n_tp), out_shape=...  34.6 us
    pallas_call x1, Pallas kernels, per_device(): pl.pallas_call(functools.partial(attend_kernel, group_heads, half_width *...  9.61 us
    unnamed x8, local copies, waits for them, and re-layouts  2.63 us
    dot_general x1, matrix products, per_device(): jnp.dot(normed, w_query.reshape(model_width, columns), preferred_element_...  1.58 us
    dot_general x1, matrix products, per_device(): jnp.dot(normed, w_key.reshape(model_width, columns), preferred_element_ty...  1.57 us

commit v1 on v0

v1 whole, which is shorter than its diff:
```python
import functools

import jax
import jax.numpy as jnp
from jax import lax
from jax.experimental import pallas as pl
from jax.experimental.pallas import tpu as pltpu
from jax.sharding import PartitionSpec as P

epsilon = 1e-06
clamp_limit = 7.0
sigmoid_slope = 1.702
branch_scale = 0.2
MESH = pl.DeviceIdType.MESH
f32, bf16 = jnp.float32, jnp.bfloat16
lane_tile = 128
wide_tile = 256
key_chunks = 4


def norm_rows(wide, gain):
    return wide * lax.rsqrt(jnp.mean(wide * wide, axis=-1, keepdims=True) + epsilon) * gain


def dot(left, right):
    return jnp.dot(left, right, preferred_element_type=f32)


def dot_rows(left, right):
    return lax.dot_general(left, right, (((1,), (1,)), ((), ())), preferred_element_type=f32)


def iota(shape, axis):
    return lax.broadcasted_iota(jnp.int32, shape, axis)


def to_column(row):
    size = row.shape[1]
    eye = iota((size, size), 0) == iota((size, size), 1)
    return jnp.sum(jnp.where(eye, row, jnp.zeros_like(row)), axis=1, keepdims=True)


def layer_kernel(
    n_ep,
    n_tp,
    n_x,
    group_heads,
    lengths_hbm,
    lambda_hbm,
    tokens_hbm,
    attn_gain_hbm,
    head_gain_hbm,
    ffn_gain_hbm,
    routes_hbm,
    route_weights_hbm,
    w_query_hbm,
    w_key_hbm,
    w_value_hbm,
    key_hbm,
    value_hbm,
    w_out_hbm,
    w_gate_hbm,
    w_up_hbm,
    w_down_hbm,
    out_ref,
    lengths_ref,
    lambda_ref,
    tokens_ref,
    attn_gain_ref,
    head_gain_ref,
    ffn_gain_ref,
    routes_ref,
    route_weights_ref,
    w_query_ref,
    w_key_ref,
    w_value_ref,
    key_ref,
    value_ref,
    w_out_ref,
    w_gate_ref,
    w_up_ref,
    w_down_ref,
    query_ref,
    score_ref,
    mix_ref,
    part_ref,
    part_in_ref,
    rows_ref,
    normed_ref,
    piece_ref,
    piece_in_ref,
    back_ref,
    back_in_ref,
    load_sems,
    key_sems,
    value_sems,
    part_sems,
    rows_sems,
    pair_sems,
    piece_sems,
    back_sems,
    sent_sems,
):
    my_ep, my_tp = lax.axis_index("ep"), lax.axis_index("tp")
    n_core = 2 if n_tp % 2 == 0 else 1
    n_y = n_tp // n_core
    n_z = n_ep // n_x
    my_y, my_core = my_tp // n_core, lax.rem(my_tp, n_core)
    my_z, my_x = my_ep // n_x, lax.rem(my_ep, n_x)
    seq_dev, model_width = tokens_ref.shape
    flat_len, head_width = key_ref.shape[1:]
    half_width = head_width // 2
    block = out_ref.shape[1]

    singles = (
        (tokens_hbm, tokens_ref),
        (attn_gain_hbm, attn_gain_ref),
        (w_query_hbm, w_query_ref),
        (w_key_hbm, w_key_ref),
        (w_value_hbm, w_value_ref),
        (lengths_hbm, lengths_ref),
        (lambda_hbm, lambda_ref),
        (head_gain_hbm, head_gain_ref),
        (ffn_gain_hbm, ffn_gain_ref),
        (routes_hbm, routes_ref),
        (route_weights_hbm, route_weights_ref),
        (w_out_hbm, w_out_ref),
        (w_gate_hbm, w_gate_ref),
        (w_up_hbm, w_up_ref),
        (w_down_hbm, w_down_ref),
    )
    loads = [
        pltpu.make_async_copy(source, target, load_sems.at[i])
        for i, (source, target) in enumerate(singles)
    ]
    chunk = flat_len // key_chunks
    key_loads = [
        pltpu.make_async_copy(
            key_hbm.at[:, pl.ds(j * chunk, chunk), :],
            key_ref.at[:, pl.ds(j * chunk, chunk), :],
            key_sems.at[j],
        )
        for j in range(key_chunks)
    ]
    pairs = seq_dev // 2
    value_loads = [
        pltpu.make_async_copy(
            value_hbm.at[pl.ds(2 * i, 2)], value_ref.at[pl.ds(2 * i, 2)], value_sems.at[i]
        )
        for i in range(pairs)
    ]
    for copy in loads[:11] + key_loads + value_loads + loads[11:]:
        copy.start()

    def device(dz, dx, dy, dc):
        ep = lax.rem(my_z + dz, n_z) * n_x + lax.rem(my_x + dx, n_x)
        tp = lax.rem(my_y + dy, n_y) * n_core + lax.rem(my_core + dc, n_core)
        return ep, tp

    def source(dz, dx, dy, dc):
        return device(n_z - dz, n_x - dx, n_y - dy, n_core - dc)

    def distance(place):
        dz, dx, dy = place
        return min(dz, n_z - dz) + min(dx, n_x - dx) + min(dy, n_y - dy)

    places = [(dz, dx, dy) for dz in range(n_z) for dx in range(n_x) for dy in range(n_y)]
    places = sorted(places, key=lambda place: -distance(place))
    remote = places[:-1]
    near_first = places[::-1]
    number = lambda place: (place[0] * n_x + place[1]) * n_y + place[2]
    tp_peers = [(dy, dc) for dy in range(n_y) for dc in range(n_core)][1:]

    barrier = pltpu.get_barrier_semaphore()
    greeted = [place + (0,) for place in remote]
    greeted += [(0, 0, dy, dc) for dy, dc in tp_peers if dc]
    for place in greeted:
        pl.semaphore_signal(barrier, inc=1, device_id=device(*place), device_id_type=MESH)

    loads[0].wait()
    loads[1].wait()
    normed = norm_rows(tokens_ref[...].astype(f32), attn_gain_ref[...]).astype(bf16)
    span = wide_tile * group_heads
    blocks = model_width // wide_tile
    stacked = jnp.concatenate(
        [normed[:, b * wide_tile : (b + 1) * wide_tile] for b in range(blocks)], axis=0
    )
    if group_heads > 1:
        spread = iota((wide_tile, span), 1) // group_heads == iota((wide_tile, span), 0)
        stacked = dot(stacked, spread.astype(f32).astype(bf16))
    else:
        stacked = stacked.astype(f32)
    lane_head = lax.rem(iota((1, span), 1), group_heads)
    left = jnp.concatenate(
        [
            jnp.concatenate(
                [
                    jnp.where(
                        lane_head == h, stacked[b * seq_dev : (b + 1) * seq_dev], 0.0
                    ).astype(bf16)
                    for h in range(group_heads)
                ],
                axis=0,
            )
            for b in range(blocks)
        ],
        axis=1,
    )
    loads[2].wait()
    queries = dot(left, w_query_ref[...]).astype(bf16).astype(f32)
    loads[3].wait()
    key_new = dot(left, w_key_ref[...]).astype(bf16).astype(f32)
    loads[4].wait()
    value_new = dot(left, w_value_ref[...]).astype(bf16).astype(f32)

    score_scale = half_width ** (-0.5)
    group_rows = group_heads * seq_dev
    first_half = iota((1, head_width), 1) < half_width
    halves = jnp.concatenate(
        [jnp.where(first_half, queries, 0.0), jnp.where(first_half, 0.0, queries)], axis=0
    )
    own = jnp.sum(halves * jnp.concatenate([key_new, key_new], axis=0), axis=-1, keepdims=True)
    own = own * score_scale
    row_seq = lax.rem(iota((2 * group_rows, 1), 0), seq_dev)
    row_head = lax.rem(iota((2 * group_rows, 1), 0) // seq_dev, group_heads)
    for s in range(seq_dev):
        query_ref[:, s * head_width : (s + 1) * head_width] = jnp.where(
            row_seq == s, halves, 0.0
        ).astype(bf16)

    for load in loads[5:11]:
        load.wait()
    limit = to_column(lengths_ref[...]) * group_heads
    limit = jnp.concatenate([limit] * (2 * group_heads), axis=0)
    balance = jnp.concatenate(
        [jnp.broadcast_to(lambda_ref[0:1, h : h + 1], (seq_dev, 1)) for h in range(group_heads)],
        axis=0,
    )

    peak = own
    for j in range(key_chunks):
        key_loads[j].wait()
        keys = jnp.concatenate(
            [key_ref[s, j * chunk : (j + 1) * chunk, :] for s in range(seq_dev)], axis=1
        )
        scores = dot_rows(query_ref[...], keys) * score_scale
        column = iota((1, chunk), 1) + j * chunk
        live = (column < limit) & (lax.rem(column, group_heads) == row_head)
        scores = jnp.where(live, scores, -jnp.inf)
        score_ref[:, j * chunk : (j + 1) * chunk] = scores
        peak = jnp.maximum(peak, jnp.max(scores, axis=-1, keepdims=True))
    own_weight = jnp.exp(own - peak)
    denominator = own_weight
    for j in range(key_chunks):
        weights = jnp.exp(score_ref[:, j * chunk : (j + 1) * chunk] - peak)
        score_ref[:, j * chunk : (j + 1) * chunk] = weights
        denominator = denominator + jnp.sum(weights, axis=-1, keepdims=True)
    inverse = 1.0 / denominator
    own_share = own_weight * inverse
    own_mix = own_share[:group_rows] - balance * own_share[group_rows:]
    own_mix = own_mix.astype(bf16).astype(f32)
    minuend, subtrahend = inverse[:group_rows], balance * inverse[group_rows:]
    for j in range(key_chunks):
        columns = slice(j * chunk, (j + 1) * chunk)
        mix_ref[:, columns] = (
            score_ref[:group_rows, columns] * minuend - score_ref[group_rows:, columns] * subtrahend
        ).astype(bf16)

    heads_out = own_mix * value_new
    group_seq = row_seq[:group_rows]
    for i in range(pairs):
        value_loads[i].wait()
        both = dot(
            mix_ref[...], jnp.concatenate([value_ref[2 * i], value_ref[2 * i + 1]], axis=1)
        )
        heads_out = heads_out + jnp.where(group_seq == 2 * i, both[:, :head_width], 0.0)
        heads_out = heads_out + jnp.where(group_seq == 2 * i + 1, both[:, head_width:], 0.0)
    heads = norm_rows(heads_out, head_gain_ref[...] * branch_scale).astype(bf16)
    heads = jnp.concatenate(
        [heads[h * seq_dev : (h + 1) * seq_dev] for h in range(group_heads)], axis=1
    )

    loads[11].wait()
    for t in range(n_tp):
        part_ref[t] = dot(heads, w_out_ref[:, t * block : (t + 1) * block]).astype(bf16)
    pl.semaphore_wait(barrier, len(greeted))

    def column_block(tp):
        return pl.ds(pl.multiple_of(tp * block, block), block)

    def row_block(ep):
        return pl.ds(pl.multiple_of(ep * seq_dev, seq_dev), seq_dev)

    for i, (dy, dc) in enumerate(tp_peers):
        peer = device(0, 0, dy, dc)
        pltpu.make_async_remote_copy(
            src_ref=part_ref.at[peer[1]],
            dst_ref=part_in_ref.at[i],
            send_sem=sent_sems.at[0],
            recv_sem=part_sems.at[0],
            device_id=peer,
            device_id_type=MESH,
        ).start()
    own_columns, own_rows = column_block(my_tp), row_block(my_ep)
    attention = part_ref[my_tp].astype(f32)
    if tp_peers:
        pltpu.make_async_copy(part_in_ref, part_in_ref, part_sems.at[0]).wait()
        for i in range(len(tp_peers)):
            attention += part_in_ref[i].astype(f32)
    residual = (tokens_ref[:, own_columns].astype(f32) + attention).astype(bf16)
    rows_ref[own_rows, own_columns] = residual

    def rows_copy(owner, peer, send, recv):
        place = rows_ref.at[row_block(owner[0]), column_block(owner[1])]
        return pltpu.make_async_remote_copy(
            src_ref=place,
            dst_ref=place,
            send_sem=send,
            recv_sem=recv,
            device_id=peer,
            device_id_type=MESH,
        )

    me = (my_ep, my_tp)
    sibling = device(0, 0, 0, 1)
    for place in remote:
        rows_copy(me, device(*place, 0), sent_sems.at[1], rows_sems.at[number(place)]).start()
    for place in near_first:
        owner = source(*place, 0)
        if place != (0, 0, 0):
            rows_copy(owner, me, sent_sems.at[1], rows_sems.at[number(place)]).wait_recv()
        if n_core > 1:
            rows_copy(owner, sibling, sent_sems.at[2], pair_sems.at[0]).start()
    if n_core > 1:
        pltpu.make_async_copy(piece_in_ref, piece_in_ref, pair_sems.at[0]).wait()

    normed_ref[...] = norm_rows(rows_ref[...].astype(f32), ffn_gain_ref[...]).astype(bf16)
    loads[12].wait()
    gate_value = jnp.minimum(dot(normed_ref[...], w_gate_ref[...]), clamp_limit)
    loads[13].wait()
    up_value = jnp.clip(dot(normed_ref[...], w_up_ref[...]), -clamp_limit, clamp_limit)
    activated = (
        (up_value + 1.0) * gate_value * jax.nn.sigmoid(sigmoid_slope * gate_value)
    ).astype(bf16)
    loads[14].wait()

    far_y = sorted(range(n_y), key=lambda dy: -min(dy, n_y - dy))
    if n_core > 1:
        for dy in far_y:
            tp = device(0, 0, dy, 1)[1]
            piece = dot(activated, w_down_ref[:, column_block(tp)]).astype(bf16)
            piece_ref[dy] = piece.reshape(n_ep, seq_dev, block)
            pltpu.make_async_remote_copy(
                src_ref=piece_ref.at[dy],
                dst_ref=piece_in_ref.at[dy],
                send_sem=sent_sems.at[3],
                recv_sem=piece_sems.at[dy],
                device_id=sibling,
                device_id_type=MESH,
            ).start()
    for dy in far_y:
        tp = device(0, 0, dy, 0)[1]
        piece = dot(activated, w_down_ref[:, column_block(tp)]).reshape(n_ep, seq_dev, block)
        if n_core > 1:
            landed = piece_in_ref.at[dy]
            pltpu.make_async_copy(landed, landed, piece_sems.at[dy]).wait()
            piece = piece + piece_in_ref[dy].astype(f32)
        back_ref[dy] = piece.astype(bf16)
        for place in remote:
            if place[2] == dy:
                peer = device(*place, 0)
                pltpu.make_async_remote_copy(
                    src_ref=back_ref.at[dy, peer[0]],
                    dst_ref=back_in_ref.at[number(place) - 1],
                    send_sem=sent_sems.at[4],
                    recv_sem=back_sems.at[number(place)],
                    device_id=peer,
                    device_id_type=MESH,
                ).start()

    total = rows_ref[own_rows, own_columns].astype(f32)
    pending = {}
    for place in near_first:
        dz, dx, dy = place
        expert = source(*place, 0)[0]
        if place == (0, 0, 0):
            value = back_ref[0, my_ep].astype(f32)
        else:
            arrived = back_in_ref.at[number(place) - 1]
            pltpu.make_async_copy(arrived, arrived, back_sems.at[number(place)]).wait()
            value = back_in_ref[number(place) - 1].astype(f32)
        count, summed = pending.get((dz, dx), (0, 0.0))
        pending[dz, dx] = (count + 1, summed + value)
        if count + 1 == n_y:
            named = jnp.where(routes_ref[...] == expert, route_weights_ref[...], 0.0)
            weight = to_column(jnp.sum(named, axis=0, keepdims=True))
            total += weight * pending[dz, dx][1].astype(bf16).astype(f32)
    out_ref[...] = total.astype(bf16)

    if tp_peers:
        pltpu.make_async_copy(part_in_ref, part_in_ref, sent_sems.at[0]).wait()
    if remote:
        pltpu.make_async_copy(back_in_ref, back_in_ref, sent_sems.at[1]).wait()
        pltpu.make_async_copy(back_in_ref, back_in_ref, sent_sems.at[4]).wait()
    if n_core > 1:
        pltpu.make_async_copy(piece_in_ref, piece_in_ref, sent_sems.at[2]).wait()
        pltpu.make_async_copy(piece_in_ref, piece_in_ref, sent_sems.at[3]).wait()


def per_device(
    tokens,
    lengths,
    key_cache,
    value_cache,
    attn_gain,
    w_query,
    w_key,
    w_value,
    mix_lambda,
    head_gain,
    w_out,
    ffn_gain,
    w_gate,
    w_up,
    w_down,
    routes,
    route_weights,
):
    n_ep, n_tp = lax.axis_size("ep"), lax.axis_size("tp")
    seq_dev, model_width = tokens.shape
    cache_len, group_heads, head_width = key_cache.shape[1:]
    flat_len = cache_len * group_heads
    group_rows = group_heads * seq_dev
    block = model_width // n_tp
    n_y = n_tp // 2 if n_tp % 2 == 0 else n_tp
    n_x = 2 ** ((n_ep.bit_length() - 1) // 2)
    n_x = n_x if n_ep % n_x == 0 else 1
    others = max(n_ep * n_y - 1, 1)
    operands = (
        lengths.reshape(1, seq_dev),
        mix_lambda.reshape(1, group_heads),
        tokens,
        attn_gain.reshape(1, model_width),
        head_gain.reshape(1, head_width),
        ffn_gain.reshape(1, model_width),
        routes.T,
        route_weights.T,
        w_query.reshape(model_width * group_heads, head_width),
        w_key.reshape(model_width * group_heads, head_width),
        w_value.reshape(model_width * group_heads, head_width),
        key_cache.reshape(seq_dev, flat_len, head_width),
        value_cache.reshape(seq_dev, flat_len, head_width),
        w_out.reshape(group_heads * head_width, model_width),
        w_gate[0],
        w_up[0],
        w_down[0],
    )
    vmem = pltpu.VMEM
    return pl.pallas_call(
        functools.partial(layer_kernel, n_ep, n_tp, n_x, group_heads),
        out_shape=jax.ShapeDtypeStruct((seq_dev, block), bf16),
        in_specs=[pl.BlockSpec(memory_space=pltpu.HBM)] * len(operands),
        out_specs=pl.BlockSpec(memory_space=vmem),
        scratch_shapes=[vmem(operand.shape, operand.dtype) for operand in operands]
        + [
            vmem((2 * group_rows, seq_dev * head_width), bf16),
            vmem((2 * group_rows, flat_len), f32),
            vmem((group_rows, flat_len), bf16),
            vmem((n_tp, seq_dev, block), bf16),
            vmem((max(n_tp - 1, 1), seq_dev, block), bf16),
            vmem((n_ep * seq_dev, model_width), bf16),
            vmem((n_ep * seq_dev, model_width), bf16),
            vmem((n_y, n_ep, seq_dev, block), bf16),
            vmem((n_y, n_ep, seq_dev, block), bf16),
            vmem((n_y, n_ep, seq_dev, block), bf16),
            vmem((others, seq_dev, block), bf16),
            pltpu.SemaphoreType.DMA((15,)),
            pltpu.SemaphoreType.DMA((key_chunks,)),
            pltpu.SemaphoreType.DMA((seq_dev // 2,)),
            pltpu.SemaphoreType.DMA((1,)),
            pltpu.SemaphoreType.DMA((n_ep * n_y,)),
            pltpu.SemaphoreType.DMA((1,)),
            pltpu.SemaphoreType.DMA((n_y,)),
            pltpu.SemaphoreType.DMA((n_ep * n_y,)),
            pltpu.SemaphoreType.DMA((5,)),
        ],
        compiler_params=pltpu.CompilerParams(
            collective_id=0, has_side_effects=True, vmem_limit_bytes=58 * 2**20
        ),
    )(*operands)


def solution(mesh):
    placed = (
        P("ep", None),
        P("ep"),
        P("ep", None, "tp", None),
        P("ep", None, "tp", None),
        P(),
        P(None, "tp", None),
        P(None, "tp", None),
        P(None, "tp", None),
        P("tp"),
        P(),
        P("tp", None, None),
        P(),
        P("ep", None, "tp"),
        P("ep", None, "tp"),
        P("ep", "tp", None),
        P("ep", None),
        P("ep", None),
    )
    return jax.shard_map(
        per_device, mesh=mesh, in_specs=placed, out_specs=P("ep", "tp"), check_vma=False
    )
```

time: 53.6 us -> 39.7 us (0.74)
  Pallas kernels: 44.2 us -> 38.1 us
  matrix products: 3.44 us -> 0 us
  local copies, waits for them, and re-layouts: 3.89 us -> 1.32 us
  other arithmetic: 1.76 us -> 0 us
    pallas_call x2 -> x1, Pallas kernels: 44.2 us -> 38.1 us  [per_device(): pl.pallas_call(functools.partial(layer_kernel, n_ep, n_tp, n_x, group_hea...]
    dot_general x3 -> x0, matrix products: 3.44 us -> none  [the longest x1 1.58 us: per_device(): jnp.dot(normed, w_query.reshape(model_width, columns), preferred_element_...]
    unnamed x8 -> x1, local copies, waits for them, and re-layouts: 2.63 us -> 1.32 us
    reduce_sum x1 -> x0, other arithmetic: 1.06 us -> none  [norm_rows(): jnp.mean(wide * wide, axis=-1, keepdims=True) + epsilon]
    another operation x1 -> x0, other arithmetic: 0.65 us -> none  [per_device(): jnp.stack([queries * halves, queries * (1 - halves)], axis=2)]
    reshape x3 -> x0, local copies, waits for them, and re-layouts: 0.64 us -> none  [the longest x1 0.61 us: per_device(): value_new = jnp.dot(normed, w_value.reshape(model_width, columns), prefer...]
    broadcast_in_dim x1 -> x0, local copies, waits for them, and re-layouts: 0.62 us -> none  [per_device(): jnp.repeat(key_new, 2, axis=1)]
where the time goes in v1:
time: 39.7 us; the launch traced here: 39.4 us
  Pallas kernels  38.1 us (96%)
  local copies, waits for them, and re-layouts  1.32 us (3%)
    pallas_call x1, Pallas kernels, per_device(): pl.pallas_call(functools.partial(layer_kernel, n_ep, n_tp, n_x, group_hea...  38.1 us
    unnamed x1, local copies, waits for them, and re-layouts  1.32 us

profile of v1, /device:TPU:0, one launch (start us, length us, event | category | flops | bytes accessed | tf_op | source)
XLA Modules:
  0.0 39.4 jit_solution(7580420505230385401)
XLA Ops:
  0.0 38.1 %shard_map.163 = bf16[16,512]{1,0:T(8,128)(2,1)} custom-call(s32[1,16]{1,0:T(1,128)} %bitcast.29, f32[1,2]{1,0:T(1,128)} %bitcast.30, bf16[16,2048]{1,0:T(8,128)(2,1)} %tokens_hbm.1, f32[1,2048]{1,0:T(1,128)} %bitcast.25, f32[1,128]{1,0:T(1,128)} %bitcast.31, f32[1,2048]{1,0:T(1,128)} %bitcast.26, s32[4,16]{1,0:T(4,128)} %bitcast.27, f32[4,16]{1,0:T(4,128)} %bitcast.28, ...), custom_call_target="tpu_custom_call" | custom-call | tf_op jit(solution)/shard_map/pallas_call | solution.py:459
  38.1 1.3 %copy.19 = bf16[16,512]{1,0:T(8,128)(2,1)} copy(bf16[16,512]{1,0:T(8,128)(2,1)} %shard_map.163) | data formatting | bytes 32768

commit v2 on v1

v2 whole, which is shorter than its diff:
```python
import functools

import jax
import jax.numpy as jnp
from jax import lax
from jax.experimental import pallas as pl
from jax.experimental.pallas import tpu as pltpu
from jax.sharding import PartitionSpec as P

epsilon = 1e-06
clamp_limit = 7.0
sigmoid_slope = 1.702
branch_scale = 0.2
MESH = pl.DeviceIdType.MESH
f32, bf16 = jnp.float32, jnp.bfloat16
lane_tile = 128
wide_tile = 256
key_chunks = 4
lent_early = 2
barrier_chunk = 2
value_chunks = 4


def norm_rows(wide, gain):
    return wide * lax.rsqrt(jnp.mean(wide * wide, axis=-1, keepdims=True) + epsilon) * gain


def dot(left, right):
    return jnp.dot(left, right, preferred_element_type=f32)


def dot_rows(left, right):
    return lax.dot_general(left, right, (((1,), (1,)), ((), ())), preferred_element_type=f32)


def iota(shape, axis):
    return lax.broadcasted_iota(jnp.int32, shape, axis)


def to_column(row):
    size = row.shape[1]
    eye = iota((size, size), 0) == iota((size, size), 1)
    return jnp.sum(jnp.where(eye, row, jnp.zeros_like(row)), axis=1, keepdims=True)


def layer_kernel(
    n_ep,
    n_tp,
    n_x,
    group_heads,
    lengths_hbm,
    lambda_hbm,
    tokens_hbm,
    attn_gain_hbm,
    head_gain_hbm,
    ffn_gain_hbm,
    routes_hbm,
    route_weights_hbm,
    w_query_hbm,
    w_key_hbm,
    w_value_hbm,
    key_hbm,
    value_hbm,
    w_out_hbm,
    w_gate_hbm,
    w_up_hbm,
    w_down_hbm,
    out_ref,
    lengths_ref,
    lambda_ref,
    tokens_ref,
    attn_gain_ref,
    head_gain_ref,
    ffn_gain_ref,
    routes_ref,
    route_weights_ref,
    w_query_ref,
    w_key_ref,
    w_value_ref,
    key_ref,
    value_ref,
    w_out_ref,
    w_gate_ref,
    w_up_ref,
    w_down_ref,
    query_ref,
    score_ref,
    mix_ref,
    part_ref,
    part_in_ref,
    residual_ref,
    rows_ref,
    back_ref,
    back_in_ref,
    load_sems,
    key_sems,
    value_sems,
    lent_sems,
    part_sems,
    rows_sems,
    back_sems,
    sent_sems,
):
    my_ep, my_tp = lax.axis_index("ep"), lax.axis_index("tp")
    n_core = 2 if n_tp % 2 == 0 and n_ep % 2 == 0 else 1
    n_y = n_tp // n_core
    n_z = n_ep // n_x
    my_y, my_core = my_tp // n_core, lax.rem(my_tp, n_core)
    my_z, my_x = my_ep // n_x, lax.rem(my_ep, n_x)
    seq_dev, model_width = tokens_ref.shape
    flat_len, head_width = key_ref.shape[1:]
    half_width = head_width // 2
    block = out_ref.shape[1]

    singles = (
        (tokens_hbm, tokens_ref),
        (attn_gain_hbm, attn_gain_ref),
        (w_query_hbm, w_query_ref),
        (w_key_hbm, w_key_ref),
        (w_value_hbm, w_value_ref),
        (lengths_hbm, lengths_ref),
        (lambda_hbm, lambda_ref),
        (head_gain_hbm, head_gain_ref),
        (ffn_gain_hbm, ffn_gain_ref),
        (routes_hbm, routes_ref),
        (route_weights_hbm, route_weights_ref),
        (w_out_hbm, w_out_ref),
        (w_gate_hbm, w_gate_ref.at[0]),
        (w_up_hbm, w_up_ref.at[0]),
        (w_down_hbm, w_down_ref.at[0]),
    )
    loads = [
        pltpu.make_async_copy(source, target, load_sems.at[i])
        for i, (source, target) in enumerate(singles)
    ]
    chunk = flat_len // key_chunks
    key_loads = [
        pltpu.make_async_copy(
            key_hbm.at[:, pl.ds(j * chunk, chunk), :],
            key_ref.at[:, pl.ds(j * chunk, chunk), :],
            key_sems.at[j],
        )
        for j in range(key_chunks)
    ]
    value_group = seq_dev // value_chunks
    value_loads = [
        pltpu.make_async_copy(
            value_hbm.at[pl.ds(i * value_group, value_group)],
            value_ref.at[pl.ds(i * value_group, value_group)],
            value_sems.at[i],
        )
        for i in range(value_chunks)
    ]
    for copy in loads[:11]:
        copy.start()
    for copy in key_loads:
        copy.start(priority=1)

    def device(dz, dx, dy, core):
        ep = lax.rem(my_z + dz, n_z) * n_x + lax.rem(my_x + dx, n_x)
        return ep, lax.rem(my_y + dy, n_y) * n_core + core

    def hops(offset):
        dz, dx = offset
        return min(dz, n_z - dz) + min(dx, n_x - dx)

    slots = sorted([(dz, dx) for dz in range(n_z) for dx in range(n_x)], key=hops)
    held = n_ep // n_core
    far_y = sorted(range(n_y), key=lambda dy: -min(dy, n_y - dy))
    far_first = [(i, dy) for i in range(n_ep)[::-1] for dy in far_y]
    tp_peers = [(dy, dc) for dy in range(n_y) for dc in range(n_core)][1:]
    sibling_core = lax.rem(my_core + 1, n_core)

    def my_offset(j):
        dz, dx = slots[j]
        for core in range(1, n_core):
            next_z, next_x = slots[j + core * held]
            last_z, last_x = slots[j + (core - 1) * held]
            past = (my_core + n_core - core) // n_core
            dz, dx = dz + (next_z - last_z) * past, dx + (next_x - last_x) * past
        return dz, dx

    barrier = pltpu.get_barrier_semaphore()
    def greet(peer):
        pl.semaphore_signal(barrier, inc=1, device_id=peer, device_id_type=MESH)

    for i, dy in far_first[:-1]:
        for core in range(n_core):
            greet(device(*slots[i], dy, core))
    for dc in range(1, n_core):
        greet(device(0, 0, 0, lax.rem(my_core + dc, n_core)))
    greeted = n_ep * n_tp - 1

    loads[0].wait()
    loads[1].wait()
    for copy in value_loads:
        copy.start(priority=1)
    normed = norm_rows(tokens_ref[...].astype(f32), attn_gain_ref[...]).astype(bf16)
    span = wide_tile * group_heads
    blocks = model_width // wide_tile
    stacked = jnp.concatenate(
        [normed[:, b * wide_tile : (b + 1) * wide_tile] for b in range(blocks)], axis=0
    )
    if group_heads > 1:
        spread = iota((wide_tile, span), 1) // group_heads == iota((wide_tile, span), 0)
        stacked = dot(stacked, spread.astype(f32).astype(bf16))
    else:
        stacked = stacked.astype(f32)
    lane_head = lax.rem(iota((1, span), 1), group_heads)
    left = jnp.concatenate(
        [
            jnp.concatenate(
                [
                    jnp.where(
                        lane_head == h, stacked[b * seq_dev : (b + 1) * seq_dev], 0.0
                    ).astype(bf16)
                    for h in range(group_heads)
                ],
                axis=0,
            )
            for b in range(blocks)
        ],
        axis=1,
    )
    loads[2].wait()
    queries = dot(left, w_query_ref[...]).astype(bf16).astype(f32)
    loads[3].wait()
    key_new = dot(left, w_key_ref[...]).astype(bf16).astype(f32)
    loads[4].wait()
    value_new = dot(left, w_value_ref[...]).astype(bf16).astype(f32)

    score_scale = half_width ** (-0.5)
    group_rows = group_heads * seq_dev
    first_half = iota((1, head_width), 1) < half_width
    halves = jnp.concatenate(
        [jnp.where(first_half, queries, 0.0), jnp.where(first_half, 0.0, queries)], axis=0
    )
    own = jnp.sum(halves * jnp.concatenate([key_new, key_new], axis=0), axis=-1, keepdims=True)
    own = own * score_scale
    row_seq = lax.rem(iota((2 * group_rows, 1), 0), seq_dev)
    row_head = lax.rem(iota((2 * group_rows, 1), 0) // seq_dev, group_heads)
    for s in range(seq_dev):
        query_ref[:, s * head_width : (s + 1) * head_width] = jnp.where(
            row_seq == s, halves, 0.0
        ).astype(bf16)

    for load in loads[5:11]:
        load.wait()
    limit = to_column(lengths_ref[...]) * group_heads
    limit = jnp.concatenate([limit] * (2 * group_heads), axis=0)
    balance = jnp.concatenate(
        [jnp.broadcast_to(lambda_ref[0:1, h : h + 1], (seq_dev, 1)) for h in range(group_heads)],
        axis=0,
    )

    def masked(j):
        columns = slice(j * chunk, (j + 1) * chunk)
        column = iota((1, chunk), 1) + j * chunk
        live = (column < limit) & (lax.rem(column, group_heads) == row_head)
        scores = jnp.where(live, score_ref[:, columns] * score_scale, -jnp.inf)
        score_ref[:, columns] = scores
        return jnp.max(scores, axis=-1, keepdims=True)

    depth = w_up_hbm.shape[0] // 2
    lent = [
        pltpu.make_async_remote_copy(
            src_ref=source,
            dst_ref=target,
            send_sem=lent_sems.at[0, i],
            recv_sem=lent_sems.at[1, i],
            device_id=device(0, 0, 0, sibling_core),
            device_id_type=MESH,
        )
        for i, (source, target) in enumerate(
            (
                (w_gate_hbm, w_gate_ref.at[n_core - 1]),
                (w_up_hbm.at[pl.ds(0, depth)], w_up_ref.at[n_core - 1, pl.ds(0, depth)]),
                (w_up_hbm.at[pl.ds(depth, depth)], w_up_ref.at[n_core - 1, pl.ds(depth, depth)]),
                (w_down_hbm, w_down_ref.at[n_core - 1]),
            )
        )
    ]
    lent = lent if n_core > 1 else []
    peak = own
    for j in range(key_chunks):
        if j == barrier_chunk:
            pl.semaphore_wait(barrier, greeted)
            for copy in lent[:lent_early]:
                copy.start()
        key_loads[j].wait()
        if j == key_chunks - 1:
            loads[11].start(priority=1)
        keys = jnp.concatenate(
            [key_ref[s, j * chunk : (j + 1) * chunk, :] for s in range(seq_dev)], axis=1
        )
        score_ref[:, j * chunk : (j + 1) * chunk] = dot_rows(query_ref[...], keys)
        if j:
            peak = jnp.maximum(peak, masked(j - 1))
    peak = jnp.maximum(peak, masked(key_chunks - 1))
    own_weight = jnp.exp(own - peak)
    denominator = own_weight
    for j in range(key_chunks):
        weights = jnp.exp(score_ref[:, j * chunk : (j + 1) * chunk] - peak)
        score_ref[:, j * chunk : (j + 1) * chunk] = weights
        denominator = denominator + jnp.sum(weights, axis=-1, keepdims=True)
    inverse = 1.0 / denominator
    own_share = own_weight * inverse
    own_mix = own_share[:group_rows] - balance * own_share[group_rows:]
    own_mix = own_mix.astype(bf16).astype(f32)
    minuend, subtrahend = inverse[:group_rows], balance * inverse[group_rows:]
    for j in range(key_chunks):
        columns = slice(j * chunk, (j + 1) * chunk)
        mix_ref[:, columns] = (
            score_ref[:group_rows, columns] * minuend - score_ref[group_rows:, columns] * subtrahend
        ).astype(bf16)

    heads_out = own_mix * value_new
    group_seq = row_seq[:group_rows]
    for i in range(value_chunks):
        value_loads[i].wait()
        if i == 0:
            for copy in loads[12:]:
                copy.start(priority=1)
        members = range(i * value_group, (i + 1) * value_group)
        values = jnp.concatenate([value_ref[s] for s in members], axis=1)
        mixed = dot(mix_ref[...], values)
        for k, s in enumerate(members):
            heads_out = heads_out + jnp.where(
                group_seq == s, mixed[:, k * head_width : (k + 1) * head_width], 0.0
            )
    heads = norm_rows(heads_out, head_gain_ref[...] * branch_scale).astype(bf16)
    heads = jnp.concatenate(
        [heads[h * seq_dev : (h + 1) * seq_dev] for h in range(group_heads)], axis=1
    )

    loads[11].wait()
    for t in range(n_tp):
        part_ref[t] = dot(heads, w_out_ref[:, t * block : (t + 1) * block]).astype(bf16)

    def column_block(tp):
        return pl.ds(pl.multiple_of(tp * block, block), block)

    def row_block(slot):
        return slice(slot * seq_dev, (slot + 1) * seq_dev)

    for i, (dy, dc) in enumerate(tp_peers):
        peer = device(0, 0, dy, lax.rem(my_core + dc, n_core))
        pltpu.make_async_remote_copy(
            src_ref=part_ref.at[peer[1]],
            dst_ref=part_in_ref.at[i],
            send_sem=sent_sems.at[0],
            recv_sem=part_sems.at[0],
            device_id=peer,
            device_id_type=MESH,
        ).start()
    own_columns = column_block(my_tp)
    attention = part_ref[my_tp].astype(f32)
    if tp_peers:
        pltpu.make_async_copy(part_in_ref, part_in_ref, part_sems.at[0]).wait()
        for i in range(len(tp_peers)):
            attention += part_in_ref[i].astype(f32)
    residual_ref[...] = (tokens_ref[:, own_columns].astype(f32) + attention).astype(bf16)

    def rows_copy(j, tp, peer, recv):
        return pltpu.make_async_remote_copy(
            src_ref=residual_ref,
            dst_ref=rows_ref.at[row_block(j), column_block(tp)],
            send_sem=sent_sems.at[1],
            recv_sem=recv,
            device_id=peer,
            device_id_type=MESH,
        )

    is_home = my_core == 0
    for i, dy in far_first:
        core, j = i // held, i % held
        copy = rows_copy(j, my_tp, device(*slots[i], dy, core), rows_sems.at[j, dy, my_core])
        if (i, dy) == (0, 0):
            pl.when(jnp.logical_not(is_home))(copy.start)
        else:
            copy.start()

    for copy in lent[lent_early:]:
        copy.start()

    @pl.when(is_home)
    def _():
        rows_ref[row_block(0), own_columns] = residual_ref[...]

    for j in range(held):
        for dy in range(n_y):
            for core in range(n_core):
                tp = device(0, 0, n_y - dy, core)[1]
                copy = rows_copy(j, tp, (my_ep, my_tp), rows_sems.at[j, dy, core])
                if (j, dy, core) == (0, 0, 0):
                    pl.when(jnp.logical_not(is_home))(copy.wait_recv)
                else:
                    copy.wait_recv()

    for load in loads[12:]:
        load.wait()
    for copy in lent:
        copy.wait_recv()
    normed = norm_rows(rows_ref[...].astype(f32), ffn_gain_ref[...]).astype(bf16)
    activated = []
    for k in range(n_core):
        gate_value = jnp.minimum(dot(normed, w_gate_ref[k]), clamp_limit)
        up_value = jnp.clip(dot(normed, w_up_ref[k]), -clamp_limit, clamp_limit)
        activated.append(
            (
                (up_value + 1.0) * gate_value * jax.nn.sigmoid(sigmoid_slope * gate_value)
            ).astype(bf16)
        )
    for dy in far_y:
        for core in range(n_core):
            columns = column_block(device(0, 0, dy, core)[1])
            share = sum(dot(activated[k], w_down_ref[k, :, columns]) for k in range(n_core))
            back_ref[dy, core] = share.astype(bf16).reshape(held, seq_dev, block)
        for j in range(held)[::-1]:
            dz, dx = my_offset(j)
            place = j + held * my_core
            for core in range(n_core):
                copy = pltpu.make_async_remote_copy(
                    src_ref=back_ref.at[dy, core, j],
                    dst_ref=back_in_ref.at[dy, place],
                    send_sem=sent_sems.at[2],
                    recv_sem=back_sems.at[place, dy],
                    device_id=device(n_z - dz, n_x - dx, dy, core),
                    device_id_type=MESH,
                )
                if (j, dy, core) == (0, 0, 0):
                    pl.when(jnp.logical_not(is_home))(copy.start)
                else:
                    copy.start()

    @pl.when(is_home)
    def _():
        back_in_ref[0, 0] = back_ref[0, 0, 0]

    total = residual_ref[...].astype(f32)
    for i in range(n_ep):
        summed = 0.0
        for dy in far_y:
            arrived = back_in_ref.at[dy, i]
            copy = pltpu.make_async_copy(arrived, arrived, back_sems.at[i, dy])
            if (i, dy) == (0, 0):
                pl.when(jnp.logical_not(is_home))(copy.wait)
            else:
                copy.wait()
            summed = summed + back_in_ref[dy, i].astype(f32)
        named = jnp.where(routes_ref[...] == device(*slots[i], 0, 0)[0], route_weights_ref[...], 0.0)
        weight = to_column(jnp.sum(named, axis=0, keepdims=True))
        total += weight * summed.astype(bf16).astype(f32)
    out_ref[...] = total.astype(bf16)

    if tp_peers:
        pltpu.make_async_copy(part_in_ref, part_in_ref, sent_sems.at[0]).wait()
    for copy in lent:
        copy.wait_send()
    every = back_in_ref.at[pl.ds(0, n_y)]
    fewer = back_in_ref.at[0, pl.ds(0, n_ep - 1)]
    rest = back_in_ref.at[pl.ds(1, n_y - 1)] if n_y > 1 else None
    for sem in (sent_sems.at[1], sent_sems.at[2]):

        @pl.when(is_home)
        def _():
            pltpu.make_async_copy(fewer, fewer, sem).wait()
            if n_y > 1:
                pltpu.make_async_copy(rest, rest, sem).wait()

        @pl.when(jnp.logical_not(is_home))
        def _():
            pltpu.make_async_copy(every, every, sem).wait()


def per_device(
    tokens,
    lengths,
    key_cache,
    value_cache,
    attn_gain,
    w_query,
    w_key,
    w_value,
    mix_lambda,
    head_gain,
    w_out,
    ffn_gain,
    w_gate,
    w_up,
    w_down,
    routes,
    route_weights,
):
    n_ep, n_tp = lax.axis_size("ep"), lax.axis_size("tp")
    seq_dev, model_width = tokens.shape
    cache_len, group_heads, head_width = key_cache.shape[1:]
    flat_len = cache_len * group_heads
    group_rows = group_heads * seq_dev
    block = model_width // n_tp
    n_core = 2 if n_tp % 2 == 0 and n_ep % 2 == 0 else 1
    n_y = n_tp // n_core
    n_x = 2 ** ((n_ep.bit_length() - 1) // 2)
    n_x = n_x if n_ep % n_x == 0 else 1
    operands = (
        lengths.reshape(1, seq_dev),
        mix_lambda.reshape(1, group_heads),
        tokens,
        attn_gain.reshape(1, model_width),
        head_gain.reshape(1, head_width),
        ffn_gain.reshape(1, model_width),
        routes.T,
        route_weights.T,
        w_query.reshape(model_width * group_heads, head_width),
        w_key.reshape(model_width * group_heads, head_width),
        w_value.reshape(model_width * group_heads, head_width),
        key_cache.reshape(seq_dev, flat_len, head_width),
        value_cache.reshape(seq_dev, flat_len, head_width),
        w_out.reshape(group_heads * head_width, model_width),
        w_gate[0],
        w_up[0],
        w_down[0],
    )
    vmem = pltpu.VMEM
    return pl.pallas_call(
        functools.partial(layer_kernel, n_ep, n_tp, n_x, group_heads),
        out_shape=pltpu.VMEM((seq_dev, block), bf16),
        in_specs=[pl.BlockSpec(memory_space=pltpu.HBM)] * len(operands),
        out_specs=pl.BlockSpec(memory_space=vmem),
        scratch_shapes=[vmem(operand.shape, operand.dtype) for operand in operands[:-3]]
        + [vmem((n_core, *operand.shape), operand.dtype) for operand in operands[-3:]]
        + [
            vmem((2 * group_rows, seq_dev * head_width), bf16),
            vmem((2 * group_rows, flat_len), f32),
            vmem((group_rows, flat_len), bf16),
            vmem((n_tp, seq_dev, block), bf16),
            vmem((max(n_tp - 1, 1), seq_dev, block), bf16),
            vmem((seq_dev, block), bf16),
            vmem((n_ep // n_core * seq_dev, model_width), bf16),
            vmem((n_y, n_core, n_ep // n_core, seq_dev, block), bf16),
            vmem((n_y, n_ep, seq_dev, block), bf16),
            pltpu.SemaphoreType.DMA((15,)),
            pltpu.SemaphoreType.DMA((key_chunks,)),
            pltpu.SemaphoreType.DMA((value_chunks,)),
            pltpu.SemaphoreType.DMA((2, 4)),
            pltpu.SemaphoreType.DMA((1,)),
            pltpu.SemaphoreType.DMA((n_ep // n_core, n_y, n_core)),
            pltpu.SemaphoreType.DMA((n_ep, n_y)),
            pltpu.SemaphoreType.DMA((3,)),
        ],
        compiler_params=pltpu.CompilerParams(
            collective_id=0, has_side_effects=True, vmem_limit_bytes=58 * 2**20
        ),
    )(*operands)


def solution(mesh):
    placed = (
        P("ep", None),
        P("ep"),
        P("ep", None, "tp", None),
        P("ep", None, "tp", None),
        P(),
        P(None, "tp", None),
        P(None, "tp", None),
        P(None, "tp", None),
        P("tp"),
        P(),
        P("tp", None, None),
        P(),
        P("ep", None, "tp"),
        P("ep", None, "tp"),
        P("ep", "tp", None),
        P("ep", None),
        P("ep", None),
    )
    return jax.shard_map(
        per_device, mesh=mesh, in_specs=placed, out_specs=P("ep", "tp"), check_vma=False
    )
```

time: 39.7 us -> 32.4 us (0.82)
  Pallas kernels: 38.1 us -> 31.6 us
  local copies, waits for them, and re-layouts: 1.32 us -> 0.61 us
    pallas_call x1, Pallas kernels: 38.1 us -> 31.6 us  [per_device(): pl.pallas_call(functools.partial(layer_kernel, n_ep, n_tp, n_x, group_hea...]
    unnamed x1, local copies, waits for them, and re-layouts: 1.32 us -> 0.61 us
where the time goes in v2:
time: 32.4 us; the launch traced here: 32.2 us
  Pallas kernels  31.6 us (98%)
  local copies, waits for them, and re-layouts  0.61 us (2%)
    pallas_call x1, Pallas kernels, per_device(): pl.pallas_call(functools.partial(layer_kernel, n_ep, n_tp, n_x, group_hea...  31.6 us

profile of v2, /device:TPU:0, one launch (start us, length us, event | category | flops | bytes accessed | tf_op | source)
XLA Modules:
  0.0 32.2 jit_solution(10550491972578494224)
XLA Ops:
  0.0 31.6 %shard_map.163 = bf16[16,512]{1,0:T(8,128)(2,1)S(1)} custom-call(s32[1,16]{1,0:T(1,128)} %bitcast.29, f32[1,2]{1,0:T(1,128)} %bitcast.30, bf16[16,2048]{1,0:T(8,128)(2,1)} %tokens_hbm.1, f32[1,2048]{1,0:T(1,128)} %bitcast.25, f32[1,128]{1,0:T(1,128)} %bitcast.31, f32[1,2048]{1,0:T(1,128)} %bitcast.26, s32[4,16]{1,0:T(4,128)} %bitcast.27, f32[4,16]{1,0:T(4,128)} %bitcast.28, ...), custom_call_target="tpu_custom_call" | custom-call | tf_op jit(solution)/shard_map/pallas_call | solution.py:525
  31.6 0.6 %copy.19 = bf16[16,512]{1,0:T(8,128)(2,1)} copy(bf16[16,512]{1,0:T(8,128)(2,1)S(1)} %shard_map.163) | data formatting | bytes 32768

commit v3 on v2

v3 whole, which is shorter than its diff:
```python
import functools

import jax
import jax.numpy as jnp
from jax import lax
from jax.experimental import pallas as pl
from jax.experimental.pallas import tpu as pltpu
from jax.sharding import PartitionSpec as P

epsilon = 1e-06
clamp_limit = 7.0
sigmoid_slope = 1.702
branch_scale = 0.2
MESH = pl.DeviceIdType.MESH
f32, bf16 = jnp.float32, jnp.bfloat16
lane_tile = 128
wide_tile = 256
waves = 2
key_chunks = 2
value_chunks = 2


def norm_rows(wide, gain):
    return wide * lax.rsqrt(jnp.mean(wide * wide, axis=-1, keepdims=True) + epsilon) * gain


def dot(left, right):
    return jnp.dot(left, right, preferred_element_type=f32)


def dot_rows(left, right):
    return lax.dot_general(left, right, (((1,), (1,)), ((), ())), preferred_element_type=f32)


def iota(shape, axis):
    return lax.broadcasted_iota(jnp.int32, shape, axis)


def to_column(row):
    size = row.shape[1]
    eye = iota((size, size), 0) == iota((size, size), 1)
    return jnp.sum(jnp.where(eye, row, jnp.zeros_like(row)), axis=1, keepdims=True)


def layer_kernel(
    n_ep,
    n_tp,
    n_x,
    group_heads,
    lengths_hbm,
    lambda_hbm,
    tokens_hbm,
    attn_gain_hbm,
    head_gain_hbm,
    ffn_gain_hbm,
    routes_hbm,
    route_weights_hbm,
    w_query_hbm,
    w_key_hbm,
    w_value_hbm,
    key_hbm,
    value_hbm,
    w_out_hbm,
    w_gate_hbm,
    w_up_hbm,
    w_down_hbm,
    out_ref,
    lengths_ref,
    lambda_ref,
    tokens_ref,
    attn_gain_ref,
    head_gain_ref,
    ffn_gain_ref,
    routes_ref,
    route_weights_ref,
    w_query_ref,
    w_key_ref,
    w_value_ref,
    key_ref,
    value_ref,
    w_out_ref,
    w_gate_ref,
    w_up_ref,
    w_down_ref,
    query_ref,
    score_ref,
    mix_ref,
    part_ref,
    part_in_ref,
    residual_ref,
    rows_ref,
    hidden_ref,
    back_ref,
    back_in_ref,
    load_sems,
    key_sems,
    value_sems,
    lent_sems,
    part_sems,
    rows_sems,
    back_sems,
    sent_sems,
):
    my_ep, my_tp = lax.axis_index("ep"), lax.axis_index("tp")
    n_core = 2 if n_tp % 2 == 0 and n_ep % 2 == 0 else 1
    n_y = n_tp // n_core
    n_z = n_ep // n_x
    my_y, my_core = my_tp // n_core, lax.rem(my_tp, n_core)
    my_z, my_x = my_ep // n_x, lax.rem(my_ep, n_x)
    seq_dev, model_width = tokens_ref.shape
    flat_len, head_width = key_ref.shape[1:]
    half_width = head_width // 2
    block = out_ref.shape[1]

    singles = (
        (tokens_hbm, tokens_ref),
        (attn_gain_hbm, attn_gain_ref),
        (w_query_hbm, w_query_ref),
        (w_key_hbm, w_key_ref),
        (w_value_hbm, w_value_ref),
        (lengths_hbm, lengths_ref),
        (lambda_hbm, lambda_ref),
        (head_gain_hbm, head_gain_ref),
        (ffn_gain_hbm, ffn_gain_ref),
        (routes_hbm, routes_ref),
        (route_weights_hbm, route_weights_ref),
        (w_out_hbm, w_out_ref),
        (w_gate_hbm, w_gate_ref.at[0]),
        (w_up_hbm, w_up_ref.at[0]),
        (w_down_hbm, w_down_ref.at[0]),
    )
    loads = [
        pltpu.make_async_copy(source, target, load_sems.at[i])
        for i, (source, target) in enumerate(singles)
    ]
    chunk = flat_len // key_chunks
    wave = seq_dev // waves
    value_group = wave // value_chunks
    key_loads = [
        [
            pltpu.make_async_copy(
                key_hbm.at[pl.ds(w * wave, wave), pl.ds(j * chunk, chunk), :],
                key_ref.at[pl.ds(w * wave, wave), pl.ds(j * chunk, chunk), :],
                key_sems.at[w, j],
            )
            for j in range(key_chunks)
        ]
        for w in range(waves)
    ]
    value_loads = [
        [
            pltpu.make_async_copy(
                value_hbm.at[pl.ds(w * wave + i * value_group, value_group)],
                value_ref.at[pl.ds(w * wave + i * value_group, value_group)],
                value_sems.at[w, i],
            )
            for i in range(value_chunks)
        ]
        for w in range(waves)
    ]

    def start_bulk(copies):
        for copy in copies:
            copy.start(priority=1)

    for copy in loads[:11]:
        copy.start()
    start_bulk(key_loads[0])

    def device(dz, dx, dy, core):
        ep = lax.rem(my_z + dz, n_z) * n_x + lax.rem(my_x + dx, n_x)
        return ep, lax.rem(my_y + dy, n_y) * n_core + core

    def hops(offset):
        dz, dx = offset
        return min(dz, n_z - dz) + min(dx, n_x - dx)

    slots = sorted([(dz, dx) for dz in range(n_z) for dx in range(n_x)], key=hops)
    held = n_ep // n_core
    far_y = sorted(range(n_y), key=lambda dy: -min(dy, n_y - dy))
    far_first = [(i, dy) for i in range(n_ep)[::-1] for dy in far_y]
    tp_peers = [(dy, dc) for dy in range(n_y) for dc in range(n_core)][1:]
    sibling_core = lax.rem(my_core + 1, n_core)

    def my_offset(j):
        dz, dx = slots[j]
        for core in range(1, n_core):
            next_z, next_x = slots[j + core * held]
            last_z, last_x = slots[j + (core - 1) * held]
            past = (my_core + n_core - core) // n_core
            dz, dx = dz + (next_z - last_z) * past, dx + (next_x - last_x) * past
        return dz, dx

    barrier = pltpu.get_barrier_semaphore()

    def greet(peer):
        pl.semaphore_signal(barrier, inc=1, device_id=peer, device_id_type=MESH)

    for i, dy in far_first[:-1]:
        for core in range(n_core):
            greet(device(*slots[i], dy, core))
    for dc in range(1, n_core):
        greet(device(0, 0, 0, lax.rem(my_core + dc, n_core)))
    greeted = n_ep * n_tp - 1

    loads[0].wait()
    loads[1].wait()
    start_bulk(value_loads[0])
    normed = norm_rows(tokens_ref[...].astype(f32), attn_gain_ref[...]).astype(bf16)
    span = wide_tile * group_heads
    blocks = model_width // wide_tile
    stacked = jnp.concatenate(
        [normed[:, b * wide_tile : (b + 1) * wide_tile] for b in range(blocks)], axis=0
    )
    if group_heads > 1:
        spread = iota((wide_tile, span), 1) // group_heads == iota((wide_tile, span), 0)
        stacked = dot(stacked, spread.astype(f32).astype(bf16))
    else:
        stacked = stacked.astype(f32)
    lane_head = lax.rem(iota((1, span), 1), group_heads)
    left = jnp.concatenate(
        [
            jnp.concatenate(
                [
                    jnp.where(
                        lane_head == h, stacked[b * seq_dev : (b + 1) * seq_dev], 0.0
                    ).astype(bf16)
                    for h in range(group_heads)
                ],
                axis=0,
            )
            for b in range(blocks)
        ],
        axis=1,
    )
    loads[2].wait()
    queries = dot(left, w_query_ref[...]).astype(bf16).astype(f32)
    loads[3].wait()
    key_new = dot(left, w_key_ref[...]).astype(bf16).astype(f32)
    loads[4].wait()
    value_new = dot(left, w_value_ref[...]).astype(bf16).astype(f32)
    start_bulk(key_loads[1])

    score_scale = half_width ** (-0.5)
    first_half = iota((1, head_width), 1) < half_width
    halves = jnp.concatenate(
        [jnp.where(first_half, queries, 0.0), jnp.where(first_half, 0.0, queries)], axis=0
    )
    own = jnp.sum(halves * jnp.concatenate([key_new, key_new], axis=0), axis=-1, keepdims=True)
    own = own * score_scale
    for load in loads[5:11]:
        load.wait()
    limit = to_column(lengths_ref[...]) * group_heads
    limit = jnp.concatenate([limit] * (2 * group_heads), axis=0)
    balance = jnp.concatenate(
        [jnp.broadcast_to(lambda_ref[0:1, h : h + 1], (wave, 1)) for h in range(group_heads)],
        axis=0,
    )
    wave_rows = group_heads * wave
    row_seq = lax.rem(iota((2 * wave_rows, 1), 0), wave)
    row_head = lax.rem(iota((2 * wave_rows, 1), 0) // wave, group_heads)

    def of_wave(rows, w):
        first = range(w * wave, rows.shape[0], seq_dev)
        return jnp.concatenate([rows[r : r + wave] for r in first], axis=0)

    depth = w_down_hbm.shape[0] // 2
    parts = ((0, depth), (depth, depth))
    lent = [
        pltpu.make_async_remote_copy(
            src_ref=source,
            dst_ref=target,
            send_sem=lent_sems.at[0, i],
            recv_sem=lent_sems.at[1, i],
            device_id=device(0, 0, 0, sibling_core),
            device_id_type=MESH,
        )
        for i, (source, target) in enumerate(
            [(w_gate_hbm, w_gate_ref.at[n_core - 1]), (w_up_hbm, w_up_ref.at[n_core - 1])]
            + [
                (w_down_hbm.at[pl.ds(*part)], w_down_ref.at[n_core - 1, pl.ds(*part)])
                for part in parts
            ]
        )
    ]
    lent = lent if n_core > 1 else []

    def lend(i):
        for copy in lent[i : i + 1]:
            copy.start()

    def share_weights(w):
        limits = of_wave(limit, w)
        own_score = of_wave(own, w)
        wave_halves = of_wave(halves, w)
        for s in range(wave):
            query_ref[w, :, s * head_width : (s + 1) * head_width] = jnp.where(
                row_seq == s, wave_halves, 0.0
            ).astype(bf16)

        def masked(j):
            columns = slice(j * chunk, (j + 1) * chunk)
            column = iota((1, chunk), 1) + j * chunk
            live = (column < limits) & (lax.rem(column, group_heads) == row_head)
            scores = jnp.where(live, score_ref[w, :, columns] * score_scale, -jnp.inf)
            score_ref[w, :, columns] = scores
            return jnp.max(scores, axis=-1, keepdims=True)

        peak = own_score
        for j in range(key_chunks):
            key_loads[w][j].wait()
            if (w, j) == (0, 0):
                loads[11].start()
                start_bulk(value_loads[1])
            keys = jnp.concatenate(
                [
                    key_ref[w * wave + s, j * chunk : (j + 1) * chunk, :]
                    for s in range(wave)
                ],
                axis=1,
            )
            score_ref[w, :, j * chunk : (j + 1) * chunk] = dot_rows(query_ref[w], keys)
            if j:
                peak = jnp.maximum(peak, masked(j - 1))
        peak = jnp.maximum(peak, masked(key_chunks - 1))
        own_weight = jnp.exp(own_score - peak)
        denominator = own_weight
        for j in range(key_chunks):
            columns = slice(j * chunk, (j + 1) * chunk)
            weights = jnp.exp(score_ref[w, :, columns] - peak)
            score_ref[w, :, columns] = weights
            denominator = denominator + jnp.sum(weights, axis=-1, keepdims=True)
        inverse = 1.0 / denominator
        own_share = own_weight * inverse
        own_mix = own_share[:wave_rows] - balance * own_share[wave_rows:]
        minuend, subtrahend = inverse[:wave_rows], balance * inverse[wave_rows:]
        for j in range(key_chunks):
            columns = slice(j * chunk, (j + 1) * chunk)
            mix_ref[w, :, columns] = (
                score_ref[w, :wave_rows, columns] * minuend
                - score_ref[w, wave_rows:, columns] * subtrahend
            ).astype(bf16)
        return own_mix.astype(bf16).astype(f32)

    def mix_values(w, own_mix, before_last):
        heads_out = own_mix * of_wave(value_new, w)
        for i in range(value_chunks):
            if i == value_chunks - 1:
                before_last()
            value_loads[w][i].wait()
            members = range(i * value_group, (i + 1) * value_group)
            values = jnp.concatenate([value_ref[w * wave + s] for s in members], axis=1)
            mixed = dot(mix_ref[w], values)
            for k, s in enumerate(members):
                heads_out = heads_out + jnp.where(
                    row_seq[:wave_rows] == s, mixed[:, k * head_width : (k + 1) * head_width], 0.0
                )
        return heads_out

    def column_block(tp):
        return pl.ds(pl.multiple_of(tp * block, block), block)

    is_home = my_core == 0
    own_columns = column_block(my_tp)

    def project(w, heads_out):
        heads = norm_rows(heads_out, head_gain_ref[...] * branch_scale)
        heads = jnp.concatenate(
            [heads[h * wave : (h + 1) * wave] for h in range(group_heads)], axis=1
        ).astype(bf16)
        for t in range(n_tp):
            part_ref[w, t] = dot(heads, w_out_ref[:, t * block : (t + 1) * block]).astype(bf16)
        for i, (dy, dc) in enumerate(tp_peers):
            peer = device(0, 0, dy, lax.rem(my_core + dc, n_core))
            pltpu.make_async_remote_copy(
                src_ref=part_ref.at[w, peer[1]],
                dst_ref=part_in_ref.at[w, i],
                send_sem=sent_sems.at[0],
                recv_sem=part_sems.at[w],
                device_id=peer,
                device_id_type=MESH,
            ).start()

    def rows_copy(w, j, tp, peer, recv):
        return pltpu.make_async_remote_copy(
            src_ref=residual_ref.at[w],
            dst_ref=rows_ref.at[w, j, tp],
            send_sem=sent_sems.at[1],
            recv_sem=recv,
            device_id=peer,
            device_id_type=MESH,
        )

    def spread_rows(w):
        attention = part_ref[w, my_tp].astype(f32)
        if tp_peers:
            landed = part_in_ref.at[w]
            pltpu.make_async_copy(landed, landed, part_sems.at[w]).wait()
            for i in range(len(tp_peers)):
                attention += part_in_ref[w, i].astype(f32)
        mine = tokens_ref[:, own_columns].astype(f32)[w * wave : (w + 1) * wave]
        residual_ref[w] = (mine + attention).astype(bf16)
        for i, dy in far_first:
            core, j = i // held, i % held
            peer = device(*slots[i], dy, core)
            copy = rows_copy(w, j, my_tp, peer, rows_sems.at[w, j, dy, my_core])
            if (i, dy) == (0, 0):
                pl.when(jnp.logical_not(is_home))(copy.start)
            else:
                copy.start()

        @pl.when(is_home)
        def _():
            rows_ref[w, 0, my_tp] = residual_ref[w]

    sources = [[(dy, core)] for core in range(n_core)[::-1] for dy in range(n_y)]

    def experts(w):
        squares = jnp.zeros((held * wave, 1), f32)
        for step, some in enumerate(sources):
            for dy, core in some:
                tp = device(0, 0, n_y - dy, core)[1]
                for j in range(held):
                    copy = rows_copy(w, j, tp, (my_ep, my_tp), rows_sems.at[w, j, dy, core])
                    if (j, dy, core) == (0, 0, 0):
                        pl.when(jnp.logical_not(is_home))(copy.wait_recv)
                    else:
                        copy.wait_recv()
            if (w, step) == (0, 0):
                for load in loads[12:14]:
                    load.wait()
                for copy in lent[:2]:
                    copy.wait_recv()
            scaled = []
            for dy, core in some:
                tp = device(0, 0, n_y - dy, core)[1]
                rows = jnp.concatenate(
                    [rows_ref[w, j, tp].astype(f32) for j in range(held)], axis=0
                )
                squares = squares + jnp.sum(rows * rows, axis=-1, keepdims=True)
                scaled.append((tp, (rows * ffn_gain_ref[:, column_block(tp)]).astype(bf16)))
            for k in range(n_core):
                for n, weight_ref in enumerate((w_gate_ref, w_up_ref)):
                    share = sum(dot(rows, weight_ref[k, column_block(tp), :]) for tp, rows in scaled)
                    if step:
                        share = share + hidden_ref[k, n]
                    hidden_ref[k, n] = share
        scale = lax.rsqrt(squares / model_width + epsilon)
        activated = []
        for k in range(n_core):
            gate_value = jnp.minimum(hidden_ref[k, 0] * scale, clamp_limit)
            up_value = jnp.clip(hidden_ref[k, 1] * scale, -clamp_limit, clamp_limit)
            activated.append(
                (
                    (up_value + 1.0) * gate_value * jax.nn.sigmoid(sigmoid_slope * gate_value)
                ).astype(bf16)
            )
        if w == 0:
            loads[14].wait()
            for copy in lent[2:]:
                copy.wait_recv()
        for dy in far_y:
            for core in range(n_core):
                columns = column_block(device(0, 0, dy, core)[1])
                share = sum(dot(activated[k], w_down_ref[k, :, columns]) for k in range(n_core))
                for j in range(held):
                    back_ref[w, dy, core, j] = share[j * wave : (j + 1) * wave].astype(bf16)
            for j in range(held)[::-1]:
                dz, dx = my_offset(j)
                place = j + held * my_core
                for core in range(n_core):
                    copy = pltpu.make_async_remote_copy(
                        src_ref=back_ref.at[w, dy, core, j],
                        dst_ref=back_in_ref.at[w, dy, place],
                        send_sem=sent_sems.at[2],
                        recv_sem=back_sems.at[w, place, dy],
                        device_id=device(n_z - dz, n_x - dx, dy, core),
                        device_id_type=MESH,
                    )
                    if (j, dy, core) == (0, 0, 0):
                        pl.when(jnp.logical_not(is_home))(copy.start)
                    else:
                        copy.start()

        @pl.when(is_home)
        def _():
            back_in_ref[w, 0, 0] = back_ref[w, 0, 0, 0]

    def collect(w, weights):
        total = residual_ref[w].astype(f32)
        for i in range(n_ep):
            summed = 0.0
            for dy in far_y:
                arrived = back_in_ref.at[w, dy, i]
                copy = pltpu.make_async_copy(arrived, arrived, back_sems.at[w, i, dy])
                if (i, dy) == (0, 0):
                    pl.when(jnp.logical_not(is_home))(copy.wait)
                else:
                    copy.wait()
                summed = summed + back_in_ref[w, dy, i].astype(f32)
            weight = weights[i][w * wave : (w + 1) * wave]
            total += weight * summed.astype(bf16).astype(f32)
        return total

    pl.semaphore_wait(barrier, greeted)
    lend(0)
    own_mix = share_weights(0)
    start_bulk(loads[12:])
    heads_out = mix_values(0, own_mix, lambda: None)
    loads[11].wait()
    project(0, heads_out)
    lend(1)
    own_mix = share_weights(1)
    heads_out = mix_values(1, own_mix, lambda: spread_rows(0))
    project(1, heads_out)
    lend(2)
    spread_rows(1)
    lend(3)
    weights = []
    for i in range(n_ep):
        named = jnp.where(routes_ref[...] == device(*slots[i], 0, 0)[0], route_weights_ref[...], 0.0)
        weights.append(to_column(jnp.sum(named, axis=0, keepdims=True)))
    experts(0)
    experts(1)
    total = jnp.concatenate([collect(w, weights) for w in range(waves)], axis=0)
    out_ref[...] = total.astype(bf16)

    if tp_peers:
        pltpu.make_async_copy(part_in_ref, part_in_ref, sent_sems.at[0]).wait()
    for copy in lent:
        copy.wait_send()
    for sem in (sent_sems.at[1], sent_sems.at[2]):
        for w in range(waves):
            fewer = back_in_ref.at[w, 0, pl.ds(0, n_ep - 1)]
            for dy in range(1, n_y):
                pltpu.make_async_copy(back_in_ref.at[w, dy], back_in_ref.at[w, dy], sem).wait()

            @pl.when(is_home)
            def _():
                pltpu.make_async_copy(fewer, fewer, sem).wait()

            @pl.when(jnp.logical_not(is_home))
            def _():
                pltpu.make_async_copy(back_in_ref.at[w, 0], back_in_ref.at[w, 0], sem).wait()


def per_device(
    tokens,
    lengths,
    key_cache,
    value_cache,
    attn_gain,
    w_query,
    w_key,
    w_value,
    mix_lambda,
    head_gain,
    w_out,
    ffn_gain,
    w_gate,
    w_up,
    w_down,
    routes,
    route_weights,
):
    n_ep, n_tp = lax.axis_size("ep"), lax.axis_size("tp")
    seq_dev, model_width = tokens.shape
    cache_len, group_heads, head_width = key_cache.shape[1:]
    flat_len = cache_len * group_heads
    wave = seq_dev // waves
    wave_rows = group_heads * wave
    block = model_width // n_tp
    n_core = 2 if n_tp % 2 == 0 and n_ep % 2 == 0 else 1
    n_y = n_tp // n_core
    n_x = 2 ** ((n_ep.bit_length() - 1) // 2)
    n_x = n_x if n_ep % n_x == 0 else 1
    operands = (
        lengths.reshape(1, seq_dev),
        mix_lambda.reshape(1, group_heads),
        tokens,
        attn_gain.reshape(1, model_width),
        head_gain.reshape(1, head_width),
        ffn_gain.reshape(1, model_width),
        routes.T,
        route_weights.T,
        w_query.reshape(model_width * group_heads, head_width),
        w_key.reshape(model_width * group_heads, head_width),
        w_value.reshape(model_width * group_heads, head_width),
        key_cache.reshape(seq_dev, flat_len, head_width),
        value_cache.reshape(seq_dev, flat_len, head_width),
        w_out.reshape(group_heads * head_width, model_width),
        w_gate[0],
        w_up[0],
        w_down[0],
    )
    vmem = pltpu.VMEM
    return pl.pallas_call(
        functools.partial(layer_kernel, n_ep, n_tp, n_x, group_heads),
        out_shape=pltpu.VMEM((seq_dev, block), bf16),
        in_specs=[pl.BlockSpec(memory_space=pltpu.HBM)] * len(operands),
        out_specs=pl.BlockSpec(memory_space=vmem),
        scratch_shapes=[vmem(operand.shape, operand.dtype) for operand in operands[:-3]]
        + [vmem((n_core, *operand.shape), operand.dtype) for operand in operands[-3:]]
        + [
            vmem((waves, 2 * wave_rows, wave * head_width), bf16),
            vmem((waves, 2 * wave_rows, flat_len), f32),
            vmem((waves, wave_rows, flat_len), bf16),
            vmem((waves, n_tp, wave, block), bf16),
            vmem((waves, max(n_tp - 1, 1), wave, block), bf16),
            vmem((waves, wave, block), bf16),
            vmem((waves, n_ep // n_core, n_tp, wave, block), bf16),
            vmem((n_core, 2, n_ep // n_core * wave, w_gate.shape[2]), f32),
            vmem((waves, n_y, n_core, n_ep // n_core, wave, block), bf16),
            vmem((waves, n_y, n_ep, wave, block), bf16),
            pltpu.SemaphoreType.DMA((15,)),
            pltpu.SemaphoreType.DMA((waves, key_chunks)),
            pltpu.SemaphoreType.DMA((waves, value_chunks)),
            pltpu.SemaphoreType.DMA((2, 4)),
            pltpu.SemaphoreType.DMA((waves,)),
            pltpu.SemaphoreType.DMA((waves, n_ep // n_core, n_y, n_core)),
            pltpu.SemaphoreType.DMA((waves, n_ep, n_y)),
            pltpu.SemaphoreType.DMA((3,)),
        ],
        compiler_params=pltpu.CompilerParams(
            collective_id=0, has_side_effects=True, vmem_limit_bytes=58 * 2**20
        ),
    )(*operands)


def solution(mesh):
    placed = (
        P("ep", None),
        P("ep"),
        P("ep", None, "tp", None),
        P("ep", None, "tp", None),
        P(),
        P(None, "tp", None),
        P(None, "tp", None),
        P(None, "tp", None),
        P("tp"),
        P(),
        P("tp", None, None),
        P(),
        P("ep", None, "tp"),
        P("ep", None, "tp"),
        P("ep", "tp", None),
        P("ep", None),
        P("ep", None),
    )
    return jax.shard_map(
        per_device, mesh=mesh, in_specs=placed, out_specs=P("ep", "tp"), check_vma=False
    )
```

time: 32.4 us -> 28.3 us (0.87)
  Pallas kernels: 31.6 us -> 27.5 us
    pallas_call x1, Pallas kernels: 31.6 us -> 27.5 us  [per_device(): pl.pallas_call(functools.partial(layer_kernel, n_ep, n_tp, n_x, group_hea...]
where the time goes in v3:
time: 28.3 us; the launch traced here: 28.1 us
  Pallas kernels  27.5 us (97%)
  local copies, waits for them, and re-layouts  0.61 us (2%)
    pallas_call x1, Pallas kernels, per_device(): pl.pallas_call(functools.partial(layer_kernel, n_ep, n_tp, n_x, group_hea...  27.5 us
    unnamed x1, local copies, waits for them, and re-layouts  0.61 us

profile of v3, /device:TPU:0, one launch (start us, length us, event | category | flops | bytes accessed | tf_op | source)
XLA Modules:
  0.0 28.1 jit_solution(12149498663263970384)
XLA Ops:
  0.0 27.5 %shard_map.163 = bf16[16,512]{1,0:T(8,128)(2,1)S(1)} custom-call(s32[1,16]{1,0:T(1,128)} %bitcast.29, f32[1,2]{1,0:T(1,128)} %bitcast.30, bf16[16,2048]{1,0:T(8,128)(2,1)} %tokens_hbm.1, f32[1,2048]{1,0:T(1,128)} %bitcast.25, f32[1,128]{1,0:T(1,128)} %bitcast.31, f32[1,2048]{1,0:T(1,128)} %bitcast.26, s32[4,16]{1,0:T(4,128)} %bitcast.27, f32[4,16]{1,0:T(4,128)} %bitcast.28, ...), custom_call_target="tpu_custom_call" | custom-call | tf_op jit(solution)/shard_map/pallas_call | solution.py:597
  27.5 0.6 %copy.19 = bf16[16,512]{1,0:T(8,128)(2,1)} copy(bf16[16,512]{1,0:T(8,128)(2,1)S(1)} %shard_map.163) | data formatting | bytes 32768

commit v4 on v3

--- a/solution.py
+++ b/solution.py
@@ -16,6 +16,8 @@
 lane_tile = 128
 wide_tile = 256
 waves = 2
+enter_chunk = 1
+lend_from = (0, 2, 4, 5, 6)
 key_chunks = 2
 value_chunks = 2
 
@@ -264,8 +266,13 @@
         first = range(w * wave, rows.shape[0], seq_dev)
         return jnp.concatenate([rows[r : r + wave] for r in first], axis=0)
 
-    depth = w_down_hbm.shape[0] // 2
-    parts = ((0, depth), (depth, depth))
+    def pieces(source, target):
+        depth = source.shape[0] // 2
+        return [
+            (source.at[pl.ds(first, depth)], target.at[n_core - 1, pl.ds(first, depth)])
+            for first in (0, depth)
+        ]
+
     lent = [
         pltpu.make_async_remote_copy(
             src_ref=source,
@@ -276,18 +283,20 @@
             device_id_type=MESH,
         )
         for i, (source, target) in enumerate(
-            [(w_gate_hbm, w_gate_ref.at[n_core - 1]), (w_up_hbm, w_up_ref.at[n_core - 1])]
-            + [
-                (w_down_hbm.at[pl.ds(*part)], w_down_ref.at[n_core - 1, pl.ds(*part)])
-                for part in parts
-            ]
+            pieces(w_gate_hbm, w_gate_ref)
+            + pieces(w_up_hbm, w_up_ref)
+            + pieces(w_down_hbm, w_down_ref)
         )
     ]
     lent = lent if n_core > 1 else []
 
-    def lend(i):
-        for copy in lent[i : i + 1]:
+    def lend(point):
+        for copy in lent[lend_from[point] : lend_from[point + 1]]:
             copy.start()
+
+    def enter():
+        pl.semaphore_wait(barrier, greeted)
+        lend(0)
 
     def share_weights(w):
         limits = of_wave(limit, w)
@@ -308,6 +317,8 @@
 
         peak = own_score
         for j in range(key_chunks):
+            if (w, j) == (0, enter_chunk):
+                enter()
             key_loads[w][j].wait()
             if (w, j) == (0, 0):
                 loads[11].start()
@@ -429,7 +440,7 @@
             if (w, step) == (0, 0):
                 for load in loads[12:14]:
                     load.wait()
-                for copy in lent[:2]:
+                for copy in lent[:4]:
                     copy.wait_recv()
             scaled = []
             for dy, core in some:
@@ -457,7 +468,7 @@
             )
         if w == 0:
             loads[14].wait()
-            for copy in lent[2:]:
+            for copy in lent[4:]:
                 copy.wait_recv()
         for dy in far_y:
             for core in range(n_core):
@@ -502,9 +513,9 @@
             total += weight * summed.astype(bf16).astype(f32)
         return total
 
-    pl.semaphore_wait(barrier, greeted)
-    lend(0)
     own_mix = share_weights(0)
+    if enter_chunk == key_chunks:
+        enter()
     start_bulk(loads[12:])
     heads_out = mix_values(0, own_mix, lambda: None)
     loads[11].wait()
@@ -615,7 +626,7 @@
             pltpu.SemaphoreType.DMA((15,)),
             pltpu.SemaphoreType.DMA((waves, key_chunks)),
             pltpu.SemaphoreType.DMA((waves, value_chunks)),
-            pltpu.SemaphoreType.DMA((2, 4)),
+            pltpu.SemaphoreType.DMA((2, 6)),
             pltpu.SemaphoreType.DMA((waves,)),
             pltpu.SemaphoreType.DMA((waves, n_ep // n_core, n_y, n_core)),
             pltpu.SemaphoreType.DMA((waves, n_ep, n_y)),

time: 28.3 us -> 27.7 us (0.979)
  Pallas kernels: 27.5 us -> 27 us
    pallas_call x1, Pallas kernels: 27.5 us -> 27 us  [per_device(): pl.pallas_call(functools.partial(layer_kernel, n_ep, n_tp, n_x, group_hea...]
where the time goes in v4:
time: 27.7 us; the launch traced here: 27.6 us
  Pallas kernels  27 us (97%)
  local copies, waits for them, and re-layouts  0.61 us (2%)
    pallas_call x1, Pallas kernels, per_device(): pl.pallas_call(functools.partial(layer_kernel, n_ep, n_tp, n_x, group_hea...  27 us
    unnamed x1, local copies, waits for them, and re-layouts  0.61 us

profile of v4, /device:TPU:0, one launch (start us, length us, event | category | flops | bytes accessed | tf_op | source)
XLA Modules:
  0.0 27.6 jit_solution(13282176201772225509)
XLA Ops:
  0.0 27.0 %shard_map.163 = bf16[16,512]{1,0:T(8,128)(2,1)S(1)} custom-call(s32[1,16]{1,0:T(1,128)} %bitcast.29, f32[1,2]{1,0:T(1,128)} %bitcast.30, bf16[16,2048]{1,0:T(8,128)(2,1)} %tokens_hbm.1, f32[1,2048]{1,0:T(1,128)} %bitcast.25, f32[1,128]{1,0:T(1,128)} %bitcast.31, f32[1,2048]{1,0:T(1,128)} %bitcast.26, s32[4,16]{1,0:T(4,128)} %bitcast.27, f32[4,16]{1,0:T(4,128)} %bitcast.28, ...), custom_call_target="tpu_custom_call" | custom-call | tf_op jit(solution)/shard_map/pallas_call | solution.py:608
  27.0 0.6 %copy.19 = bf16[16,512]{1,0:T(8,128)(2,1)} copy(bf16[16,512]{1,0:T(8,128)(2,1)S(1)} %shard_map.163) | data formatting | bytes 32768

commit v5 on v4

--- a/solution.py
+++ b/solution.py
@@ -17,7 +17,7 @@
 wide_tile = 256
 waves = 2
 enter_chunk = 1
-lend_from = (0, 2, 4, 5, 6)
+lend_from = (0, 2, 4, 6, 6)
 key_chunks = 2
 value_chunks = 2
 
@@ -470,12 +470,19 @@
             loads[14].wait()
             for copy in lent[4:]:
                 copy.wait_recv()
+        returned = {}
         for dy in far_y:
             for core in range(n_core):
                 columns = column_block(device(0, 0, dy, core)[1])
-                share = sum(dot(activated[k], w_down_ref[k, :, columns]) for k in range(n_core))
+                returned[dy, core] = sum(
+                    dot(activated[k], w_down_ref[k, :, columns]) for k in range(n_core)
+                )
+        for dy in far_y:
+            for core in range(n_core):
                 for j in range(held):
-                    back_ref[w, dy, core, j] = share[j * wave : (j + 1) * wave].astype(bf16)
+                    back_ref[w, dy, core, j] = returned[dy, core][
+                        j * wave : (j + 1) * wave
+                    ].astype(bf16)
             for j in range(held)[::-1]:
                 dz, dx = my_offset(j)
                 place = j + held * my_core

time: 27.7 us -> 27.7 us (level)
  no operation moved by 1% of the time
where the time goes in v5:
time: 27.7 us; the launch traced here: 27.6 us
  Pallas kernels  26.9 us (97%)
  local copies, waits for them, and re-layouts  0.61 us (2%)
    pallas_call x1, Pallas kernels, per_device(): pl.pallas_call(functools.partial(layer_kernel, n_ep, n_tp, n_x, group_hea...  26.9 us
    unnamed x1, local copies, waits for them, and re-layouts  0.61 us

profile of v5, /device:TPU:0, one launch (start us, length us, event | category | flops | bytes accessed | tf_op | source)
XLA Modules:
  0.0 27.6 jit_solution(8679701157870864921)
XLA Ops:
  0.0 26.9 %shard_map.163 = bf16[16,512]{1,0:T(8,128)(2,1)S(1)} custom-call(s32[1,16]{1,0:T(1,128)} %bitcast.29, f32[1,2]{1,0:T(1,128)} %bitcast.30, bf16[16,2048]{1,0:T(8,128)(2,1)} %tokens_hbm.1, f32[1,2048]{1,0:T(1,128)} %bitcast.25, f32[1,128]{1,0:T(1,128)} %bitcast.31, f32[1,2048]{1,0:T(1,128)} %bitcast.26, s32[4,16]{1,0:T(4,128)} %bitcast.27, f32[4,16]{1,0:T(4,128)} %bitcast.28, ...), custom_call_target="tpu_custom_call" | custom-call | tf_op jit(solution)/shard_map/pallas_call | solution.py:615
  26.9 0.6 %copy.19 = bf16[16,512]{1,0:T(8,128)(2,1)} copy(bf16[16,512]{1,0:T(8,128)(2,1)S(1)} %shard_map.163) | data formatting | bytes 32768
